TPU v7x, 512 devices: a whole 4x8x8 slice. The times are simulated.
512 devices in a mesh: sp: 32 (over z, x), tp: 16 (over y, core).
Axes of the slice: x: 4, y: 8, z: 8, core: 2. Of those that a mesh axis runs over, the one named last changes fastest.
Arguments:
- stream: bfloat16 [4096, 2048], P('sp'), may hold values from -15 to 15
- cotangent: bfloat16 [4096, 2048], P('sp'), may hold values from -6 to 6
- route_ids: int32 [4096, 2], P('sp'), may hold values from 0 to 31, all different within a row; in each aligned block of 128 rows (0 to 127, 128 to 255, ...) at most 16 rows name the same one
- route_weights: float32 [4096, 2], P('sp'), may hold values from 0.1 to 0.9
- w_gate: bfloat16 [32, 2048, 2048], P('sp', None, 'tp'), may hold values from -0.125 to 0.125
- w_up: bfloat16 [32, 2048, 2048], P('sp', None, 'tp'), may hold values from -0.125 to 0.125
- w_down: bfloat16 [32, 2048, 2048], P('sp', 'tp'), may hold values from -0.125 to 0.125
- out_proj: bfloat16 [2048, 512], P(None, 'tp'), may hold values from -0.25 to 0.25
- mixed: bfloat16 [512, 4096], P('tp', 'sp'), may hold values from -6 to 6
- rec_input: bfloat16 [512, 4096], P('tp', 'sp'), may hold values from -6 to 6
- branch_input: bfloat16 [512, 4096], P('tp', 'sp'), may hold values from -6 to 6
- state_before: float32 [512, 4096], P('tp', 'sp'), may hold values from -6 to 6
- rec_gates: bfloat16 [16, 32, 32], P('tp'), may hold values from -1 to 1
- in_gates: bfloat16 [16, 32, 32], P('tp'), may hold values from -1 to 1
- decay_param: float32 [512], P('tp'), may hold values from 4.4 to 11
- decay_shift: float32 [512, 4096], P('tp', 'sp'), may hold values from -1.4 to -1e-05
Outputs:
- grad_gate: bfloat16 [32, 2048, 2048], P('sp', None, 'tp')
- grad_up: bfloat16 [32, 2048, 2048], P('sp', None, 'tp')
- grad_down: bfloat16 [32, 2048, 2048], P('sp', 'tp')
- grad_proj: float32 [2048, 512], P('sp', 'tp')
- grad_rec: float32 [512, 4096], P('tp', 'sp')
- grad_branch: float32 [512, 4096], P('tp', 'sp')
Inputs may be any that keep to these rules, and one draw needn't show every extreme that they name: `route_ids`: each row names 2 different experts; the rows of one device name no expert more than 16 times, a bound that some block reaches on some device.
All inputs are finite; a program needn't handle non-finite values.
Results may differ from a plain program's by a relative error of at most 0.03.
Values may be sent and summed in bfloat16 or wider, within the bound.
No kernel may reach another device: no remote copies, remote signals or barrier semaphores. Data moves between devices by JAX's collectives and lax.ppermute only.
A program may use at most 64 MiB of HBM per device.

v0:
```python
import jax
import jax.numpy as jnp
from jax import lax
from jax.sharding import PartitionSpec as P

RATE_SCALE = 8.0
CLAMP_LIMIT = 7.0
GLU_ALPHA = 1.702


def in_one_piece(arrays, axis, split_dim, concat_dim, along):
    widths = [a.shape[along] for a in arrays]
    both = jnp.concatenate(arrays, axis=along)
    filled = lax.all_to_all(both, axis, split_axis=split_dim, concat_axis=concat_dim, tiled=True)
    return tuple(jnp.split(filled, [sum(widths[:k]) for k in range(1, len(widths))], axis=along))


def split_up(array, dim, size):
    before, after = (array.shape[:dim], array.shape[dim + 1 :])
    return jnp.moveaxis(array.reshape(*before, size, -1, *after), dim, 0)


def sum_at_owner(array, axis, dim):
    size = lax.axis_size(axis)
    tiles = lax.all_to_all(split_up(array, dim, size), axis, 0, 0, tiled=True)
    return jnp.sum(tiles.astype(jnp.float32), axis=0)


def sent_to_all(array, axis):
    size = lax.axis_size(axis)
    return lax.all_to_all(
        jnp.broadcast_to(array[None], (size, *array.shape)), axis, 0, 0, tiled=True
    )


def all_in_one(array, axis):
    leaves = jax.tree.leaves(array)
    order = sorted(range(len(leaves)), key=lambda k: -leaves[k].size)
    width = (1, *leaves[order[0]].shape)[-1]
    lines = [
        jnp.pad(leaves[k].reshape(-1), (0, -leaves[k].size % width)).reshape(-1, width)
        for k in order
    ]
    both, at, found = (sent_to_all(jnp.concatenate(lines), axis), 0, {})
    for k, line in zip(order, lines):
        slab = both[:, at : at + len(line)].reshape(len(both), -1)
        found[k] = slab[:, : leaves[k].size].reshape(-1, *leaves[k].shape)
        at += len(line)
    numbers = iter(range(len(leaves)))
    return jax.tree.map(lambda _: found[next(numbers)], array)


def folded_in_pairs(pieces, combine):
    while len(jax.tree.leaves(pieces)[0]) > 1:
        pieces = jax.vmap(combine)(
            *(jax.tree.map(lambda part: part[side::2], pieces) for side in (0, 1))
        )
    return jax.tree.map(lambda part: part[0], pieces)


def carried_in(array, axis, combine, identity):
    size, position = (lax.axis_size(axis), lax.axis_index(axis))
    passed = jnp.arange(size) > position

    def kept(part, zero, own):
        part = jnp.where(
            passed.reshape(-1, *(1 for _ in own.shape)), part, jnp.asarray(zero, own.dtype)
        )
        return part[::-1]

    pieces = all_in_one(array, axis)
    return folded_in_pairs(jax.tree.map(kept, pieces, identity, array), combine)


def expert_act(gate_pre, up_pre):
    glu_part = jnp.minimum(gate_pre, CLAMP_LIMIT)
    lin_part = jnp.clip(up_pre, -CLAMP_LIMIT, CLAMP_LIMIT)
    return glu_part * jax.nn.sigmoid(GLU_ALPHA * glu_part) * (lin_part + 1.0)


def reverse_step(later_elem, earlier_elem):
    return (later_elem[0] * earlier_elem[0], earlier_elem[1] + earlier_elem[0] * later_elem[1])


def compose_maps(higher_map, lower_map):
    return (lower_map[0] * higher_map[0], lower_map[0] * higher_map[1] + lower_map[1])


def weight_grads(tokens_in, grads_in, d_gate, d_up, act_low):
    g_gate = jnp.einsum("secd,secf->edf", tokens_in, d_gate, preferred_element_type=jnp.float32)
    g_up = jnp.einsum("secd,secf->edf", tokens_in, d_up, preferred_element_type=jnp.float32)
    g_down = jnp.einsum("secf,secd->efd", act_low, grads_in, preferred_element_type=jnp.float32)
    return (g_gate.astype(jnp.bfloat16), g_up.astype(jnp.bfloat16), g_down.astype(jnp.bfloat16))


def local(
    stream,
    cotangent,
    route_ids,
    route_weights,
    w_gate,
    w_up,
    w_down,
    out_proj,
    mixed,
    rec_input,
    branch_input,
    state_before,
    rec_gates,
    in_gates,
    decay_param,
    decay_shift,
):
    sp_count = lax.axis_size("sp")
    tok_rows, model_width = cotangent.shape
    top_count = route_ids.shape[1]
    local_experts = w_gate.shape[0]
    expert_count = local_experts * sp_count
    capacity = 2 * tok_rows * top_count // expert_count
    flat_ids = route_ids.reshape(-1)
    onehot = (flat_ids[:, None] == jnp.arange(expert_count, dtype=jnp.int32)[None, :]).astype(
        jnp.int32
    )
    slot_index = jnp.sum((jnp.cumsum(onehot, axis=0) - onehot) * onehot, axis=1)
    target = flat_ids * capacity + slot_index
    scaled = (route_weights[:, :, None] * cotangent[:, None, :].astype(jnp.float32)).astype(
        jnp.bfloat16
    )
    scaled = scaled.reshape(-1, model_width)
    copies = jnp.broadcast_to(stream[:, None, :], (tok_rows, top_count, model_width)).reshape(
        -1, model_width
    )
    empty_rows = jnp.zeros((expert_count * capacity, model_width), jnp.bfloat16)
    rows_sent = empty_rows.at[target].set(scaled)
    tokens_sent = empty_rows.at[target].set(copies)
    grads_in, tokens_in = in_one_piece((rows_sent, tokens_sent), "sp", 0, 0, 1)
    grads_in = grads_in.reshape(sp_count, local_experts, capacity, model_width)
    tokens_in = tokens_in.reshape(sp_count, local_experts, capacity, model_width)
    gate_pre = jnp.einsum("secd,edf->secf", tokens_in, w_gate, preferred_element_type=jnp.float32)
    up_pre = jnp.einsum("secd,edf->secf", tokens_in, w_up, preferred_element_type=jnp.float32)
    act_val, act_vjp = jax.vjp(expert_act, gate_pre, up_pre)
    act_low = act_val.astype(jnp.bfloat16)
    d_act = jnp.einsum("secd,efd->secf", grads_in, w_down, preferred_element_type=jnp.float32)
    d_gate, d_up = act_vjp(d_act)
    d_gate = d_gate.astype(jnp.bfloat16)
    d_up = d_up.astype(jnp.bfloat16)
    grad_gate, grad_up, grad_down = weight_grads(tokens_in, grads_in, d_gate, d_up, act_low)
    partial_value = jnp.einsum("secf,edf->secd", d_gate, w_gate, preferred_element_type=jnp.float32)
    partial_value = partial_value + jnp.einsum(
        "secf,edf->secd", d_up, w_up, preferred_element_type=jnp.float32
    )
    share = sum_at_owner(partial_value.astype(jnp.bfloat16), "tp", 3).astype(jnp.bfloat16)
    share_cols = share.shape[3]
    returned = lax.all_to_all(
        share.reshape(-1, share_cols), "sp", split_axis=0, concat_axis=0, tiled=True
    )
    per_pair = returned[target].astype(jnp.float32).reshape(tok_rows, top_count, share_cols)
    own_cols = lax.dynamic_slice_in_dim(cotangent, lax.axis_index("tp") * share_cols, share_cols, 1)
    share_low = (own_cols.astype(jnp.float32) + jnp.sum(per_pair, axis=1)).astype(jnp.bfloat16)
    stream_low = lax.all_gather(share_low, "tp", axis=1, tiled=True)
    d_mixed = lax.dot_general(
        out_proj, stream_low, (((0,), (1,)), ((), ())), preferred_element_type=jnp.float32
    )
    grad_proj = sum_at_owner(
        lax.dot_general(
            stream_low, mixed, (((0,), (1,)), ((), ())), preferred_element_type=jnp.float32
        ).astype(jnp.bfloat16),
        "sp",
        0,
    )
    channels, positions = rec_input.shape
    gate_heads = rec_gates.shape[0]
    head_dim = rec_gates.shape[1]
    rec_heads = rec_input.reshape(gate_heads, head_dim, positions)
    rec_pre = jnp.einsum(
        "hij,hit->hjt", rec_gates, rec_heads, preferred_element_type=jnp.float32
    ).reshape(channels, positions)
    in_pre = jnp.einsum(
        "hij,hit->hjt", in_gates, rec_heads, preferred_element_type=jnp.float32
    ).reshape(channels, positions)
    rec_gate = jax.nn.sigmoid(rec_pre)
    in_gate = jax.nn.sigmoid(in_pre)
    soft_plus = jax.nn.softplus(-decay_param)[:, None]
    log_decay = -RATE_SCALE * rec_gate * soft_plus + decay_shift
    decay_rate = jnp.exp(log_decay)
    token_position = lax.axis_index("sp") * positions + jnp.arange(positions, dtype=jnp.int32)
    at_start = (token_position == 0)[None, :]
    raw_mult = jnp.sqrt(-jnp.expm1(2.0 * log_decay))
    multiplier = jnp.where(at_start, 1.0, raw_mult)
    rec_value = rec_input.astype(jnp.float32)
    state_now = decay_rate * state_before + multiplier * in_gate * rec_value
    gelu_val, gelu_vjp = jax.vjp(jax.nn.gelu, branch_input.astype(jnp.float32))
    grad_branch = gelu_vjp(d_mixed * state_now)[0]
    d_state = d_mixed * gelu_val
    next_decay = jnp.concatenate([decay_rate[:, 1:], jnp.zeros((channels, 1), jnp.float32)], axis=1)
    local_adj = lax.associative_scan(reverse_step, (next_decay, d_state), reverse=True, axis=1)[1]
    log_cumsum = jnp.cumsum(log_decay, axis=1)
    total_log = log_cumsum[:, -1:]
    tail_decay = jnp.exp(total_log - log_cumsum)
    device_prod = jnp.exp(total_log[:, 0])
    head_term = decay_rate[:, 0] * local_adj[:, 0]
    identity = (jnp.ones((channels,), jnp.float32), jnp.zeros((channels,), jnp.float32))
    carried = carried_in((device_prod, head_term), "sp", compose_maps, identity)
    adjoint = local_adj + tail_decay * carried[1][:, None]
    mult_term = adjoint * in_gate * rec_value * decay_rate * decay_rate / raw_mult
    d_log = adjoint * state_before * decay_rate - jnp.where(at_start, 0.0, mult_term)
    d_rec_pre = (d_log * -RATE_SCALE * soft_plus * rec_gate * (1.0 - rec_gate)).astype(jnp.bfloat16)
    d_in_pre = (adjoint * multiplier * rec_value * in_gate * (1.0 - in_gate)).astype(jnp.bfloat16)
    back_rec = jnp.einsum(
        "hij,hjt->hit",
        rec_gates,
        d_rec_pre.reshape(gate_heads, head_dim, positions),
        preferred_element_type=jnp.float32,
    )
    back_in = jnp.einsum(
        "hij,hjt->hit",
        in_gates,
        d_in_pre.reshape(gate_heads, head_dim, positions),
        preferred_element_type=jnp.float32,
    )
    grad_rec = adjoint * multiplier * in_gate + (back_rec + back_in).reshape(channels, positions)
    return (grad_gate, grad_up, grad_down, grad_proj, grad_rec, grad_branch)


def solution(mesh):
    placed = (
        P("sp", None),
        P("sp", None),
        P("sp", None),
        P("sp", None),
        P("sp", None, "tp"),
        P("sp", None, "tp"),
        P("sp", "tp", None),
        P(None, "tp"),
        P("tp", "sp"),
        P("tp", "sp"),
        P("tp", "sp"),
        P("tp", "sp"),
        P("tp", None, None),
        P("tp", None, None),
        P("tp"),
        P("tp", "sp"),
    )
    return jax.shard_map(
        local,
        mesh=mesh,
        in_specs=placed,
        out_specs=(
            P("sp", None, "tp"),
            P("sp", None, "tp"),
            P("sp", "tp", None),
            P("sp", "tp"),
            P("tp", "sp"),
            P("tp", "sp"),
        ),
        check_vma=False,
    )
```

profile of v0, /device:TPU:1, one launch (start us, length us, event | category | flops | bytes accessed | tf_op | source)
XLA Modules:
  0.0 272.0 jit_solution(11788468494152365258)
XLA Ops:
  0.7 0.8 broadcast_multiply_fusion
  1.4 0.8 copy.57
  2.8 0.6 reduce-window.6
  3.6 1.7 broadcast_in_dim.63
  5.3 1.2 reshape.294
  6.5 2.4 mul.322
  8.9 2.7 mul.323
  12.0 4.4 %scatter_custom_fusion.1 = bf16[512,2048]{1,0:T(8,128)(2,1)} fusion(s32[256]{0:T(256)S(1)} %bitcast.230, bf16[256,2048]{1,0:T(8,128)(2,1)} %reshape.294, bf16[]{:T(256)} %constant.21.clone.1), kind=kCustom, calls=%fused_computation.33 | custom fusion | bytes 2097664 | tf_op jit(solution)/shard_map/scatter | solution.py:135
  16.4 3.8 %scatter_custom_fusion = bf16[512,2048]{1,0:T(8,128)(2,1)} fusion(s32[256]{0:T(256)S(1)} %bitcast.231, f32[256,2048]{1,0:T(8,128)S(1)} %mul.323, f32[256]{0:T(256)S(1)} %mul.320, bf16[]{:T(256)} %constant.21.clone.1), kind=kCustom, calls=%fused_computation.31 | custom fusion | flops 1048576 | bytes 4195330 | tf_op jit(solution)/shard_map/scatter | solution.py:134
  20.2 2.7 pad_maximum_fusion
  22.9 107.1 %all_to_all.36 = bf16[32,16,4096]{2,1,0:T(8,128)(2,1)S(1)} all-to-all(bf16[32,16,4096]{2,1,0:T(8,128)(2,1)S(1)} %bitcast.217), channel_id=1, replica_groups=mesh['sp'=32,'tp'=16] {'sp'}, dimensions={0} | all-to-all | bytes 8388608 | tf_op jit(solution)/shard_map/all_to_all | solution.py:14
  130.0 0.4 fusion.103
  130.4 0.6 copy-done.3
  131.0 0.7 fusion.25
  131.8 0.7 fusion.22
  132.5 0.3 copy-done.12
  132.8 0.8 fusion.33
  133.7 0.7 fusion.20
  134.4 0.7 fusion.6
  135.1 1.9 copy.70
  137.0 10.1 %all-to-all-start.1 = ((bf16[16,32,1,16,128]{4,3,1,2,0:T(8,128)(2,1)}), bf16[16,32,1,16,128]{4,3,1,2,0:T(8,128)(2,1)}, u32[]{:S(2)}, u32[]{:S(2)}) async-start(bf16[16,32,1,16,128]{4,3,1,2,0:T(8,128)(2,1)} %bitcast.218), calls=%async_computation.1 | async-start | bytes 4194304 | tf_op jit(solution)/shard_map/all_to_all | solution.py:25
  147.5 1.6 fusion.4
  149.1 47.1 %all-to-all-done.1 = bf16[16,32,1,16,128]{4,3,1,2,0:T(8,128)(2,1)} async-done(((bf16[16,32,1,16,128]{4,3,1,2,0:T(8,128)(2,1)}), bf16[16,32,1,16,128]{4,3,1,2,0:T(8,128)(2,1)}, u32[]{:S(2)}, u32[]{:S(2)}) %all-to-all-start.1) | async-done | bytes 2097184 | tf_op jit(solution)/shard_map/all_to_all | solution.py:25
  196.2 2.6 reduce_sum.43
  198.8 5.3 %all-to-all-start.2 = ((bf16[32,16,128]{2,1,0:T(8,128)(2,1)}), bf16[32,16,128]{2,1,0:T(8,128)(2,1)S(1)}, u32[]{:S(2)}, u32[]{:S(2)}) async-start(bf16[32,16,128]{2,1,0:T(8,128)(2,1)} %reduce_sum.43), calls=%async_computation.2 | async-start | bytes 262144 | tf_op jit(solution)/shard_map/all_to_all | solution.py:154
  204.1 1.6 fusion.3
  205.7 1.3 fusion.5
  207.0 6.5 %all-to-all-done.2 = bf16[32,16,128]{2,1,0:T(8,128)(2,1)S(1)} async-done(((bf16[32,16,128]{2,1,0:T(8,128)(2,1)}), bf16[32,16,128]{2,1,0:T(8,128)(2,1)S(1)}, u32[]{:S(2)}, u32[]{:S(2)}) %all-to-all-start.2) | async-done | bytes 131104 | tf_op jit(solution)/shard_map/all_to_all | solution.py:154
  213.5 0.9 gather_fusion
  214.6 0.8 add_convert_fusion.1
  215.4 18.7 %all_gather.3 = bf16[128,2048]{1,0:T(8,128)(2,1)S(1)} all-gather(bf16[128,128]{1,0:T(8,128)(2,1)S(1)} %add_convert_fusion.1), channel_id=1, replica_groups=mesh['sp'=32,'tp'=16] {'tp'}, dimensions={1}, use_global_device_ids=true | all-gather | bytes 557056 | tf_op jit(solution)/shard_map/all_gather | solution.py:160
  234.1 0.9 fusion.54
  235.1 0.3 slice.281
  235.5 0.3 slice.291
  235.8 0.3 slice.285
  236.1 0.3 slice.278
  236.5 0.3 slice.283
  236.8 0.3 slice.287
  243.6 0.3 pad.56
  243.9 0.3 pad.57
  244.7 0.6 broadcast_in_dim.65
  245.3 3.8 %all-to-all-start.4 = ((f32[32,2,32]{2,1,0:T(2,128)}), f32[32,2,32]{2,1,0:T(2,128)S(1)}, u32[]{:S(2)}, u32[]{:S(2)}) async-start(f32[32,2,32]{2,1,0:T(2,128)} %broadcast_in_dim.65), calls=%async_computation.4 | async-start | bytes 65536 | tf_op jit(solution)/shard_map/all_to_all | solution.py:31
  249.7 0.8 reshape.312
  250.6 7.2 %all-to-all-done.4 = f32[32,2,32]{2,1,0:T(2,128)S(1)} async-done(((f32[32,2,32]{2,1,0:T(2,128)}), f32[32,2,32]{2,1,0:T(2,128)S(1)}, u32[]{:S(2)}, u32[]{:S(2)}) %all-to-all-start.4) | async-done | bytes 8224 | tf_op jit(solution)/shard_map/all_to_all | solution.py:31
  257.8 3.9 %all-to-all-start.3 = ((bf16[32,2,1024]{2,1,0:T(2,128)(2,1)}), bf16[32,2,1024]{2,1,0:T(2,128)(2,1)S(1)}, u32[]{:S(2)}, u32[]{:S(2)}) async-start(bf16[32,2,1024]{2,1,0:T(2,128)(2,1)} %reshape.312), calls=%async_computation.3 | async-start | bytes 262144 | tf_op jit(solution)/shard_map/all_to_all | solution.py:25
  262.4 0.8 fusion.8
  263.2 7.9 %all-to-all-done.3 = bf16[32,2,1024]{2,1,0:T(2,128)(2,1)S(1)} async-done(((bf16[32,2,1024]{2,1,0:T(2,128)(2,1)}), bf16[32,2,1024]{2,1,0:T(2,128)(2,1)S(1)}, u32[]{:S(2)}, u32[]{:S(2)}) %all-to-all-start.3) | async-done | bytes 131104 | tf_op jit(solution)/shard_map/all_to_all | solution.py:25
  271.3 0.7 convert_reduce_fusion
  (160 shorter events, 9.9 us)
Async XLA Ops:
  0.6 131.1 %copy-start = (bf16[1,2048,128]{2,1,0:T(8,128)(2,1)S(1)}, bf16[1,2048,128]{2,1,0:T(8,128)(2,1)}, u32[]{:S(2)}) copy-start(bf16[1,2048,128]{2,1,0:T(8,128)(2,1)} %param.20) | copy-start | bytes 1572868
  0.6 5.9 %copy-start.4 = (bf16[128,2048]{1,0:T(8,128)(2,1)S(1)}, bf16[128,2048]{1,0:T(8,128)(2,1)}, u32[]{:S(2)}) copy-start(bf16[128,2048]{1,0:T(8,128)(2,1)} %param.17) | copy-start | bytes 1572868
  8.9 2.7 copy-start.11
  130.0 1.0 copy-start.3
  130.4 2.1 copy-start.1
  131.8 1.0 copy-start.12
  137.0 10.1 %copy-start.15 = (f32[32]{0:T(128)S(1)}, f32[32]{0:T(128)}, u32[]{:S(2)}) copy-start(f32[32]{0:T(128)} %param.30) | copy-start | bytes 388
  137.0 10.1 %copy-start.9 = (bf16[32,128]{1,0:T(8,128)(2,1)S(1)}, bf16[32,128]{1,0:T(8,128)(2,1)}, u32[]{:S(2)}) copy-start(bf16[32,128]{1,0:T(8,128)(2,1)} %param.25) | copy-start | bytes 24580
  137.0 10.1 %copy-start.13 = (bf16[1,32,32]{2,1,0:T(8,128)(2,1)S(1)}, bf16[1,32,32]{2,1,0:T(8,128)(2,1)}, u32[]{:S(2)}) copy-start(bf16[1,32,32]{2,1,0:T(8,128)(2,1)} %param.28) | copy-start | bytes 6148
  137.0 10.3 %copy-start.14 = (bf16[1,32,32]{2,1,0:T(8,128)(2,1)S(1)}, bf16[1,32,32]{2,1,0:T(8,128)(2,1)}, u32[]{:S(2)}) copy-start(bf16[1,32,32]{2,1,0:T(8,128)(2,1)} %param.29) | copy-start | bytes 6148
  137.0 59.2 %all-to-all-start.1 = ((bf16[16,32,1,16,128]{4,3,1,2,0:T(8,128)(2,1)}), bf16[16,32,1,16,128]{4,3,1,2,0:T(8,128)(2,1)}, u32[]{:S(2)}, u32[]{:S(2)}) async-start(bf16[16,32,1,16,128]{4,3,1,2,0:T(8,128)(2,1)} %bitcast.218), calls=%async_computation.1 | async-start | bytes 4194304 | tf_op jit(solution)/shard_map/all_to_all | solution.py:25
  198.8 14.8 %all-to-all-start.2 = ((bf16[32,16,128]{2,1,0:T(8,128)(2,1)}), bf16[32,16,128]{2,1,0:T(8,128)(2,1)S(1)}, u32[]{:S(2)}, u32[]{:S(2)}) async-start(bf16[32,16,128]{2,1,0:T(8,128)(2,1)} %reduce_sum.43), calls=%async_computation.2 | async-start | bytes 262144 | tf_op jit(solution)/shard_map/all_to_all | solution.py:154
  204.1 1.6 copy-start.2
  205.7 28.4 %copy-start.5 = (bf16[2048,32]{0,1:T(8,128)(2,1)S(1)}, bf16[2048,32]{0,1:T(8,128)(2,1)}, u32[]{:S(2)}) copy-start(bf16[2048,32]{0,1:T(8,128)(2,1)} %param.23) | copy-start | bytes 393220
  205.7 28.4 %copy-start.6 = (f32[32,128]{1,0:T(8,128)S(1)}, f32[32,128]{1,0:T(8,128)}, u32[]{:S(2)}) copy-start(f32[32,128]{1,0:T(8,128)} %param.31) | copy-start | bytes 49156
  205.7 28.4 %copy-start.7 = (f32[32,128]{1,0:T(8,128)S(1)}, f32[32,128]{1,0:T(8,128)}, u32[]{:S(2)}) copy-start(f32[32,128]{1,0:T(8,128)} %param.27) | copy-start | bytes 49156
  205.7 28.4 %copy-start.8 = (bf16[32,128]{1,0:T(8,128)(2,1)S(1)}, bf16[32,128]{1,0:T(8,128)(2,1)}, u32[]{:S(2)}) copy-start(bf16[32,128]{1,0:T(8,128)(2,1)} %param.26) | copy-start | bytes 24580
  235.0 14.1 %copy-start.10 = (bf16[32,128]{1,0:T(8,128)(2,1)S(1)}, bf16[32,128]{1,0:T(8,128)(2,1)}, u32[]{:S(2)}) copy-start(bf16[32,128]{1,0:T(8,128)(2,1)} %param.24) | copy-start | bytes 24580
  245.3 12.5 %all-to-all-start.4 = ((f32[32,2,32]{2,1,0:T(2,128)}), f32[32,2,32]{2,1,0:T(2,128)S(1)}, u32[]{:S(2)}, u32[]{:S(2)}) async-start(f32[32,2,32]{2,1,0:T(2,128)} %broadcast_in_dim.65), calls=%async_computation.4 | async-start | bytes 65536 | tf_op jit(solution)/shard_map/all_to_all | solution.py:31
  257.8 13.3 %all-to-all-start.3 = ((bf16[32,2,1024]{2,1,0:T(2,128)(2,1)}), bf16[32,2,1024]{2,1,0:T(2,128)(2,1)S(1)}, u32[]{:S(2)}, u32[]{:S(2)}) async-start(bf16[32,2,1024]{2,1,0:T(2,128)(2,1)} %reshape.312), calls=%async_computation.3 | async-start | bytes 262144 | tf_op jit(solution)/shard_map/all_to_all | solution.py:25
where the time goes:
time: 273 us; the launch traced here: 272 us
  blocking collectives  126 us (46%)
  waiting for transfers between devices  68.8 us (25%)
  local copies, waits for them, and re-layouts  28.7 us (11%)
  starting transfers between devices  23 us (8%)
  other arithmetic  13.6 us (5%)
  matrix products  10.7 us (4%)
    all_to_all x1, blocking collectives, in_one_piece(): lax.all_to_all(both, axis, split_axis=split_dim, concat_axis=concat_dim,...  107 us
    all_to_all x2, waiting for transfers between devices, sum_at_owner(): tiles = lax.all_to_all(split_up(array, dim, size), axis, 0, 0, tiled=True)  55 us
    all_gather x1, blocking collectives, local(): stream_low = lax.all_gather(share_low, 'tp', axis=1, tiled=True)  18.7 us
    all_to_all x2, starting transfers between devices, sum_at_owner(): tiles = lax.all_to_all(split_up(array, dim, size), axis, 0, 0, tiled=True)  13.9 us
    all_to_all x1, waiting for transfers between devices, sent_to_all(): lax.all_to_all(jnp.broadcast_to(array[None], (size, *array.shape)), axis,...  7.21 us
    all_to_all x1, waiting for transfers between devices, local(): lax.all_to_all(share.reshape(-1, share_cols), 'sp', split_axis=0, concat_...  6.53 us
    slice x41, local copies, waits for them, and re-layouts, local(): lax.associative_scan(reverse_step, (next_decay, d_state), reverse=True, a...  5.9 us
  transfers between devices with their start and end apart: 4, of which 4 were waited for; matrix products, arithmetic and copies ran while one was open for 3% of the time, Pallas kernels for 0%

commit v1 on v0

v1 whole, which is shorter than its diff:
```python
import functools

import jax
import jax.numpy as jnp
from jax import lax
from jax.experimental import pallas as pl
from jax.experimental.pallas import tpu as pltpu
from jax.sharding import PartitionSpec as P

RATE_SCALE = 8.0
CLAMP_LIMIT = 7.0
GLU_ALPHA = 1.702
F32 = jnp.float32
BF16 = jnp.bfloat16
GROUP = 4
SUB = 4


def dot(a, b, ca=1, cb=0):
    return lax.dot_general(a, b, (((ca,), (cb,)), ((), ())), preferred_element_type=F32)


def call(body, out, *args, flops=0, scratch=(), specs=None):
    out = tuple(out) if isinstance(out, (list, tuple)) else out
    return pl.pallas_call(
        body,
        out_shape=out,
        in_specs=specs if specs else [pl.BlockSpec(memory_space=pltpu.VMEM)] * len(args),
        scratch_shapes=list(scratch),
        cost_estimate=pl.CostEstimate(flops=flops, bytes_accessed=1 << 20, transcendentals=0),
    )(*args)


def sds(shape, dtype):
    return jax.ShapeDtypeStruct(shape, dtype)


def iota(shape, dim):
    return lax.broadcasted_iota(jnp.int32, shape, dim)


def pack_body(g_ref, u_ref, d_ref, o_ref):
    o_ref[:, 0:128] = g_ref[...]
    o_ref[:, 128:256] = u_ref[...]
    for j in range(d_ref.shape[1] // 128):
        o_ref[128 * j : 128 * (j + 1), 256:384] = d_ref[:, 128 * j : 128 * (j + 1)].T


def pack(w_gate, w_up, w_down):
    return call(pack_body, sds((w_gate.shape[0], 384), BF16), w_gate, w_up, w_down, flops=1 << 20)


def route_body(ids_ref, w_ref, stream_ref, cot_ref, o_ref):
    tok = stream_ref.shape[0]
    rows = o_ref.shape[0]
    sub = lax.axis_index("tp") % GROUP
    line = iota((rows, tok), 0)
    expert = line // 8
    slot = line % SUB + sub * SUB
    is_grad = (line % 8) >= SUB

    def along_lanes(ref, k):
        one = jnp.broadcast_to(ref[:, k : k + 1], (tok, tok)).T
        return jnp.concatenate([one] * (rows // tok), axis=0)

    first = along_lanes(ids_ref, 0) == expert
    second = along_lanes(ids_ref, 1) == expert
    named = first | second
    before = dot(
        jnp.where(named, 1.0, 0.0).astype(BF16),
        jnp.where(iota((tok, tok), 0) < iota((tok, tok), 1), 1.0, 0.0).astype(BF16),
    )
    here = named & (before == slot.astype(F32))
    weight = jnp.where(first, along_lanes(w_ref, 0), along_lanes(w_ref, 1))
    weight = jnp.sum(jnp.where(here & is_grad, weight, 0.0), axis=1, keepdims=True)
    weight = jnp.where(is_grad[:, 0:1], weight, 1.0)
    pick_x = jnp.where(here & ~is_grad, 1.0, 0.0).astype(BF16)
    pick_g = jnp.where(here & is_grad, 1.0, 0.0).astype(BF16)
    for j in range(stream_ref.shape[1] // 512):
        cols = slice(512 * j, 512 * (j + 1))
        both = dot(pick_x, stream_ref[:, cols]) + dot(pick_g, cot_ref[:, cols])
        o_ref[:, cols] = (both * weight).astype(BF16)


def expert_body(r_ref, *refs):
    weights, (o_ref, z_ref, buf, acc, sems) = refs[:GROUP], refs[GROUP:]
    rows = r_ref.shape[0]
    copies = [pltpu.make_async_copy(weights[k], buf.at[k], sems.at[k]) for k in range(GROUP)]
    for copy in copies:
        copy.start()
    is_x = (iota((rows, 128), 0) % 8) < SUB
    half = rows // 2
    want = iota((half, rows), 0)
    pick = (want // SUB) * 8 + want % SUB == iota((half, rows), 1)
    pick = jnp.where(pick, 1.0, 0.0).astype(BF16)
    for k in range(GROUP):
        copies[k].wait()
        pre = dot(r_ref[...], buf[k])
        gate, up = pre[:, 0:128], pre[:, 128:256]
        d_act = pltpu.roll(pre[:, 256:384], rows - SUB, 0)
        glu = jnp.minimum(gate, CLAMP_LIMIT)
        lin = jnp.clip(up, -CLAMP_LIMIT, CLAMP_LIMIT) + 1.0
        sig = jax.nn.sigmoid(GLU_ALPHA * glu)
        swish = glu * sig
        act = swish * lin
        slope = lin * (sig + GLU_ALPHA * swish * (1.0 - sig))
        d_gate = jnp.where(is_x & (gate <= CLAMP_LIMIT), d_act * slope, 0.0)
        d_up = jnp.where(is_x & (jnp.abs(up) <= CLAMP_LIMIT), d_act * swish, 0.0)
        act = jnp.where(is_x, 0.0, pltpu.roll(act, SUB, 0))
        d_both = jnp.concatenate([d_gate, d_up], axis=1).astype(BF16)
        z_ref[k, :, 0:256] = d_both
        z_ref[k, :, 256:384] = act.astype(BF16)
        d_rows = dot(pick, d_both).astype(BF16)
        part = dot(d_rows, buf[k, :, 0:256], 1, 1)
        if k == 0:
            acc[...] = part
        elif k < GROUP - 1:
            acc[...] += part
        else:
            total = acc[...] + part
            for j in range(o_ref.shape[0]):
                o_ref[j] = total[:, 128 * j : 128 * (j + 1)].astype(BF16)


def grads_body(r_ref, z_ref, own_ref, other_ref):
    turned = r_ref[...].T
    for ref, at, k in ((other_ref, 0, 1), (other_ref, 1, 3), (own_ref, 0, 0), (own_ref, 1, 2)):
        ref[at] = dot(turned, z_ref[k]).astype(BF16)


def combine_body(ids_ref, recv_ref, own_ref, o_ref):
    tok = own_ref.shape[0]
    lanes = recv_ref.shape[0] // GROUP
    col = iota((tok, lanes), 1)
    per_sub = lanes // GROUP
    slot = (col // per_sub) * SUB + col % SUB
    expert = (col % per_sub) // SUB
    named = (ids_ref[:, 0:1] == expert) | (ids_ref[:, 1:2] == expert)
    before = dot(
        jnp.where(iota((tok, tok), 0) > iota((tok, tok), 1), 1.0, 0.0).astype(BF16),
        jnp.where(named, 1.0, 0.0).astype(BF16),
    )
    pick = jnp.where(named & (before == slot.astype(F32)), 1.0, 0.0).astype(BF16)
    total = own_ref[...].astype(F32)
    for k in range(GROUP):
        total = total + dot(pick, recv_ref[lanes * k : lanes * (k + 1)])
    o_ref[...] = total.astype(BF16)


def in_three(x):
    high = x.astype(BF16)
    rest = x - high.astype(F32)
    mid = rest.astype(BF16)
    return high, mid, (rest - mid.astype(F32)).astype(BF16)


def scan_body(s_ref, proj_ref, mixed_ref, fac_ref, pay_ref, gb_ref, adj_ref, tail_ref):
    ch, tok = mixed_ref.shape
    blocks = s_ref.shape[0]
    low = iota((16, 128), 1) < 64
    d_mixed = jnp.zeros((ch, tok), F32)
    for j in range(blocks):
        s = s_ref[j]
        d_mixed = d_mixed + dot(proj_ref[:, 128 * j : 128 * (j + 1)], s, 1, 1)
        g = dot(mixed_ref[...], s)
        a, b = g[0:16], g[16:32]
        pay_ref[2 * j, 0:16] = jnp.where(low, a, pltpu.roll(b, 64, 1)).astype(BF16)
        pay_ref[2 * j + 1, 0:16] = jnp.where(low, pltpu.roll(a, 64, 1), b).astype(BF16)
    decay = fac_ref[0]
    gb_ref[...] = d_mixed * fac_ref[2]
    at = iota((ch, tok), 1)
    val = d_mixed * fac_ref[1]
    mul = jnp.where(at < tok - 1, pltpu.roll(decay, tok - 1, 1), 1.0)
    step = 1
    while step < tok:
        inside = at < tok - step
        later_val = jnp.where(inside, pltpu.roll(val, tok - step, 1), 0.0)
        later_mul = jnp.where(inside, pltpu.roll(mul, tok - step, 1), 1.0)
        val = val + mul * later_val
        mul = mul * later_mul
        step *= 2
    adj_ref[...] = val
    tail_ref[...] = mul
    first = at == 0
    head = jnp.sum(jnp.where(first, decay * val, 0.0), axis=1, keepdims=True)
    prod = jnp.sum(jnp.where(first, decay * mul, 0.0), axis=1, keepdims=True)
    cols = jnp.where(first, prod, jnp.where(at == 1, head, 0.0))
    cols = jnp.concatenate([cols, jnp.zeros((tok - ch, tok), F32)], axis=0)
    lines = cols.T[0:8]
    high, mid, rest = in_three(lines)
    lines = (
        high.astype(F32)
        + pltpu.roll(mid.astype(F32), 32, 1)
        + pltpu.roll(rest.astype(F32), 64, 1)
    ).astype(BF16)
    for k in range(pay_ref.shape[0]):
        pay_ref[k, 16:24] = lines


def finish_body(recv_ref, adj_ref, tail_ref, fac_ref, rg_ref, ig_ref, gp_ref, gr_ref):
    count = recv_ref.shape[0]
    me = lax.axis_index("sp")
    total = recv_ref[0, 0:16].astype(F32)
    for k in range(1, count):
        total = total + recv_ref[k, 0:16].astype(F32)
    turned = total.T
    gp_ref[:, 0:16] = turned[0:64]
    gp_ref[:, 16:32] = turned[64:128]
    carried = jnp.zeros((1, 128), F32)
    for k in range(count - 1, -1, -1):
        x = recv_ref[k, 16:24].astype(F32)
        x = x + pltpu.roll(x, 96, 1) + pltpu.roll(x, 64, 1)
        new = x[1:2] + x[0:1] * carried
        carried = jnp.where(k > me, new, carried)
    ch = adj_ref.shape[0]
    carried = jnp.broadcast_to(carried, (128, 128)).T[0:ch]
    adj = adj_ref[...] + tail_ref[...] * carried
    d_rec = (adj * fac_ref[3]).astype(BF16)
    d_in = (adj * fac_ref[4]).astype(BF16)
    gr_ref[...] = adj * fac_ref[5] + dot(rg_ref[...], d_rec) + dot(ig_ref[...], d_in)


def unpack_body(a_ref, b_ref, g_ref, u_ref, d_ref):
    for j in range(a_ref.shape[0] // 128):
        lines = slice(128 * j, 128 * (j + 1))
        total = a_ref[lines].astype(F32) + b_ref[lines].astype(F32)
        total = total.astype(BF16)
        g_ref[lines] = total[:, 0:128]
        u_ref[lines] = total[:, 128:256]
        d_ref[:, lines] = total[:, 256:384].T


def add_body(own_ref, got_ref, keep_ref, pass_ref):
    for ref, k in ((pass_ref, 1), (keep_ref, 0)):
        ref[...] = (own_ref[k].astype(F32) + got_ref[k].astype(F32)).astype(BF16)


def recurrence_factors(rec_input, branch_input, state_before, rec_gates, in_gates, decay_param, decay_shift):
    channels, positions = rec_input.shape
    rec_pre = dot(rec_gates, rec_input, 0, 0)
    in_pre = dot(in_gates, rec_input, 0, 0)
    rec_gate = jax.nn.sigmoid(rec_pre)
    in_gate = jax.nn.sigmoid(in_pre)
    soft_plus = jax.nn.softplus(-decay_param)[:, None]
    log_decay = -RATE_SCALE * rec_gate * soft_plus + decay_shift
    decay = jnp.exp(log_decay)
    at_start = (lax.axis_index("sp") * positions + jnp.arange(positions, dtype=jnp.int32) == 0)[None, :]
    raw_mult = jnp.sqrt(-jnp.expm1(2.0 * log_decay))
    multiplier = jnp.where(at_start, 1.0, raw_mult)
    rec_value = rec_input.astype(F32)
    state_now = decay * state_before + multiplier * in_gate * rec_value
    gelu_val, gelu_vjp = jax.vjp(jax.nn.gelu, branch_input.astype(F32))
    branch = gelu_vjp(state_now)[0]
    mult_term = jnp.where(at_start, 0.0, in_gate * rec_value * decay * decay / raw_mult)
    d_log = state_before * decay - mult_term
    d_rec = d_log * (-RATE_SCALE * soft_plus) * rec_gate * (1.0 - rec_gate)
    d_in = multiplier * rec_value * in_gate * (1.0 - in_gate)
    return jnp.stack([decay, gelu_val, branch, d_rec, d_in, multiplier * in_gate])


def local(
    stream,
    cotangent,
    route_ids,
    route_weights,
    w_gate,
    w_up,
    w_down,
    out_proj,
    mixed,
    rec_input,
    branch_input,
    state_before,
    rec_gates,
    in_gates,
    decay_param,
    decay_shift,
):
    sp_count, tp_count = lax.axis_size("sp"), lax.axis_size("tp")
    tok, width = cotangent.shape
    core = [(i, i ^ 1) for i in range(tp_count)]
    chip = [(i, i ^ 2) for i in range(tp_count)]

    own = pack(w_gate[0], w_up[0], w_down[0])
    across = lax.ppermute(own, "tp", chip)
    beside = lax.ppermute(own, "tp", core)
    rows = call(
        route_body,
        sds((sp_count * 8, width), BF16),
        route_ids,
        route_weights,
        stream,
        cotangent,
        flops=1 << 28,
    )
    recv = lax.all_to_all(rows.reshape(sp_count, 8, width), "sp", 0, 0, tiled=True)
    recv = recv.reshape(sp_count * 8, width)
    across_beside = lax.ppermute(across, "tp", core)
    vmem, hbm = pl.BlockSpec(memory_space=pltpu.VMEM), pl.BlockSpec(memory_space=pl.ANY)
    slots = sp_count * SUB
    terms, kept = call(
        expert_body,
        (sds((tp_count, slots, 128), BF16), sds((GROUP, sp_count * 8, 384), BF16)),
        recv,
        own,
        beside,
        across,
        across_beside,
        flops=1 << 31,
        specs=[vmem] + [hbm] * GROUP,
        scratch=(
            pltpu.VMEM((GROUP, width, 384), BF16),
            pltpu.VMEM((slots, width), F32),
            pltpu.SemaphoreType.DMA((GROUP,)),
        ),
    )
    back = lax.all_to_all(
        terms.reshape(tp_count * sp_count, SUB, 128), ("tp", "sp"), 0, 0, tiled=True
    ).reshape(-1, 128)
    grads_own, grads_other = call(
        grads_body,
        (sds((2, width, 384), BF16), sds((2, width, 384), BF16)),
        recv,
        kept,
        flops=1 << 31,
    )
    got = lax.ppermute(grads_other, "tp", core)
    keep, send = call(
        add_body, (sds((width, 384), BF16), sds((width, 384), BF16)), grads_own, got, flops=1 << 27
    )
    arrived = lax.ppermute(send, "tp", chip)

    own_cols = lax.dynamic_slice_in_dim(cotangent, lax.axis_index("tp") * 128, 128, 1)
    share = call(combine_body, sds((tok, 128), BF16), route_ids, back, own_cols, flops=1 << 27)
    low = lax.all_gather(share, "tp", axis=0)
    factors = recurrence_factors(
        rec_input, branch_input, state_before, rec_gates[0], in_gates[0], decay_param, decay_shift
    )
    channels = mixed.shape[0]
    plane = sds((channels, tok), F32)
    payload, grad_branch, adj, tail = call(
        scan_body,
        (sds((sp_count, 24, 128), BF16), plane, plane, plane),
        low,
        out_proj.T,
        mixed,
        factors,
        flops=1 << 27,
    )
    final = lax.all_to_all(payload, "sp", 0, 0, tiled=True)
    grad_proj, grad_rec = call(
        finish_body,
        (sds((width // sp_count, channels), F32), plane),
        final,
        adj,
        tail,
        factors,
        rec_gates[0],
        in_gates[0],
        flops=1 << 25,
    )
    grad_gate, grad_up, grad_down = call(
        unpack_body,
        (sds((width, 128), BF16), sds((width, 128), BF16), sds((128, width), BF16)),
        keep,
        arrived,
        flops=1 << 27,
    )
    return (grad_gate[None], grad_up[None], grad_down[None], grad_proj, grad_rec, grad_branch)


def solution(mesh):
    placed = (
        P("sp", None),
        P("sp", None),
        P("sp", None),
        P("sp", None),
        P("sp", None, "tp"),
        P("sp", None, "tp"),
        P("sp", "tp", None),
        P(None, "tp"),
        P("tp", "sp"),
        P("tp", "sp"),
        P("tp", "sp"),
        P("tp", "sp"),
        P("tp", None, None),
        P("tp", None, None),
        P("tp"),
        P("tp", "sp"),
    )
    return jax.shard_map(
        local,
        mesh=mesh,
        in_specs=placed,
        out_specs=(
            P("sp", None, "tp"),
            P("sp", None, "tp"),
            P("sp", "tp", None),
            P("sp", "tp"),
            P("tp", "sp"),
            P("tp", "sp"),
        ),
        check_vma=False,
    )
```

time: 273 us -> 184 us (0.67)
  blocking collectives: 126 us -> 61 us
  waiting for transfers between devices: 68.8 us -> 23.7 us
  Pallas kernels: 0 us -> 35.4 us
  starting transfers between devices: 23 us -> 53.1 us
  local copies, waits for them, and re-layouts: 28.7 us -> 8.17 us
  other arithmetic: 13.6 us -> 0.17 us
  matrix products: 10.7 us -> 0.38 us
    all_to_all x1, blocking collectives: 107 us -> 22.1 us  [local(): final = lax.all_to_all(payload, 'sp', 0, 0, tiled=True)]
    all_to_all x4 -> x2, waiting for transfers between devices: 68.8 us -> 15 us  [the longest x1 8.8 us: local(): lax.all_to_all(terms.reshape(tp_count * sp_count, SUB, 128), ('tp', 'sp')...]
    pallas_call x0 -> x9, Pallas kernels: none -> 35.4 us  [call(): pl.pallas_call(body, out_shape=out, in_specs=specs if specs else [pl.Bloc...]
    ppermute x0 -> x5, starting transfers between devices: none -> 23.4 us  [the longest x1 7.96 us: local(): across_beside = lax.ppermute(across, 'tp', core)]
    all_gather x1, blocking collectives: 18.7 us -> 39 us  [local(): low = lax.all_gather(share, 'tp', axis=0)]
    dot_general x14 -> x2, matrix products: 10.7 us -> 0.38 us  [dot(): lax.dot_general(a, b, (((ca,), (cb,)), ((), ())), preferred_element_type=...]
    ppermute x0 -> x5, waiting for transfers between devices: none -> 8.7 us  [the longest x1 8.69 us: local(): across = lax.ppermute(own, 'tp', chip)]
    slice x65 -> x0, local copies, waits for them, and re-layouts: 6.7 us -> none  [the longest x41 5.9 us: local(): lax.associative_scan(reverse_step, (next_decay, d_state), reverse=True, a...]
  transfers between devices with their start and end apart: 4 -> 7, of which waited for: 4 -> 3; matrix products, arithmetic and copies ran while one was open for 3% -> 3% of each run, Pallas kernels for 0% -> 8%
where the time goes in v1:
time: 184 us; the launch traced here: 183 us
  blocking collectives  61 us (33%)
  starting transfers between devices  53.1 us (29%)
  Pallas kernels  35.4 us (19%)
  waiting for transfers between devices  23.7 us (13%)
  local copies, waits for them, and re-layouts  8.17 us (4%)
    all_gather x1, blocking collectives, local(): low = lax.all_gather(share, 'tp', axis=0)  39 us
    pallas_call x9, Pallas kernels, call(): pl.pallas_call(body, out_shape=out, in_specs=specs if specs else [pl.Bloc...  35.4 us
    all_to_all x1, blocking collectives, local(): final = lax.all_to_all(payload, 'sp', 0, 0, tiled=True)  22.1 us
    all_to_all x1, starting transfers between devices, local(): lax.all_to_all(terms.reshape(tp_count * sp_count, SUB, 128), ('tp', 'sp')...  16.6 us
    all_to_all x1, starting transfers between devices, local(): lax.all_to_all(rows.reshape(sp_count, 8, width), 'sp', 0, 0, tiled=True)  13 us
    all_to_all x1, waiting for transfers between devices, local(): lax.all_to_all(terms.reshape(tp_count * sp_count, SUB, 128), ('tp', 'sp')...  8.8 us
    ppermute x1, waiting for transfers between devices, local(): across = lax.ppermute(own, 'tp', chip)  8.69 us
    ppermute x1, starting transfers between devices, local(): across_beside = lax.ppermute(across, 'tp', core)  7.96 us
  transfers between devices with their start and end apart: 7, of which 3 were waited for; matrix products, arithmetic and copies ran while one was open for 3% of the time, Pallas kernels for 8%

profile of v1, /device:TPU:1, one launch (start us, length us, event | category | flops | bytes accessed | tf_op | source)
XLA Modules:
  0.0 182.9 jit_solution(2287691929591018077)
XLA Ops:
  0.6 0.0 copy-start.10
  0.6 0.0 copy-start.11
  0.7 2.9 %shard_map.200.refs_0_ = bf16[2048,384]{1,0:T(8,128)(2,1)} custom-call(bf16[2048,128]{1,0:T(8,128)(2,1)} %bitcast.47, bf16[2048,128]{1,0:T(8,128)(2,1)} %bitcast.48, bf16[128,2048]{1,0:T(8,128)(2,1)} %bitcast.49), custom_call_target="tpu_custom_call" | custom-call | flops 1048576 | bytes 1048576 | tf_op jit(solution)/shard_map/pallas_call | solution.py:25
  3.5 4.0 %collective-permute-start.1 = (bf16[2048,384]{1,0:T(8,128)(2,1)}, bf16[2048,384]{1,0:T(8,128)(2,1)}, u32[]{:S(2)}, u32[]{:S(2)}) collective-permute-start(bf16[2048,384]{1,0:T(8,128)(2,1)} %shard_map.200.refs_0_), channel_id=1, source_target_pairs={{0,2},{1,3},{2,0},{3,1},{4,6},{5,7},{6,4},{7,5},{8,10},{9,11},{10,... | collective-permute-start | bytes 4718600 | tf_op jit(solution)/shard_map/ppermute | solution.py:285
  7.6 0.0 copy-done.10
  7.6 0.7 copy.22.ids_ref
  8.3 0.0 copy-done.11
  8.3 0.7 copy.23.w_ref
  9.1 3.2 %shard_map.199 = bf16[256,2048]{1,0:T(8,128)(2,1)} custom-call(s32[128,2]{1,0:T(8,128)} %copy.22.ids_ref, f32[128,2]{1,0:T(8,128)} %copy.23.w_ref, bf16[128,2048]{1,0:T(8,128)(2,1)} %stream_ref.1, bf16[128,2048]{1,0:T(8,128)(2,1)} %cot_ref.1), custom_call_target="tpu_custom_call" | custom-call | flops 268435456 | bytes 1048576 | tf_op jit(solution)/shard_map/pallas_call | solution.py:25
  12.3 13.0 %all-to-all-start = ((bf16[32,8,2048]{2,1,0:T(8,128)(2,1)}), bf16[32,8,2048]{2,1,0:T(8,128)(2,1)S(1)}, u32[]{:S(2)}, u32[]{:S(2)}) async-start(bf16[32,8,2048]{2,1,0:T(8,128)(2,1)} %bitcast.42), calls=%async_computation | async-start | bytes 2097152 | tf_op jit(solution)/shard_map/all_to_all | solution.py:296
  25.3 3.2 %collective-permute-start = (bf16[2048,384]{1,0:T(8,128)(2,1)S(1)}, bf16[2048,384]{1,0:T(8,128)(2,1)}, u32[]{:S(2)}, u32[]{:S(2)}) collective-permute-start(bf16[2048,384]{1,0:T(8,128)(2,1)S(1)} %copy-done.2), channel_id=1, source_target_pairs={{0,1},{1,0},{2,3},{3,2},{4,5},{5,4},{6,7},{7,6},{8,9},{9,8},{10,11... | collective-permute-start | bytes 4718600 | tf_op jit(solution)/shard_map/ppermute | solution.py:286
  28.5 8.7 %collective-permute-done.1.refs_2_ = bf16[2048,384]{1,0:T(8,128)(2,1)} collective-permute-done((bf16[2048,384]{1,0:T(8,128)(2,1)}, bf16[2048,384]{1,0:T(8,128)(2,1)}, u32[]{:S(2)}, u32[]{:S(2)}) %collective-permute-start.1) | collective-permute-done | bytes 1572896 | tf_op jit(solution)/shard_map/ppermute | solution.py:285
  37.1 8.0 %collective-permute-start.2 = (bf16[2048,384]{1,0:T(8,128)(2,1)}, bf16[2048,384]{1,0:T(8,128)(2,1)}, u32[]{:S(2)}, u32[]{:S(2)}) collective-permute-start(bf16[2048,384]{1,0:T(8,128)(2,1)} %collective-permute-done.1.refs_2_), channel_id=1, source_target_pairs={{0,1},{1,0},{2,3},{3,2},{4,5},{5,4},{6,7},{7,6},{8,9},{9,8},{10,11... | collective-permute-start | bytes 4718600 | tf_op jit(solution)/shard_map/ppermute | solution.py:298
  45.1 0.0 collective-permute-done.refs_1_
  45.1 6.2 %all-to-all-done = bf16[32,8,2048]{2,1,0:T(8,128)(2,1)S(1)} async-done(((bf16[32,8,2048]{2,1,0:T(8,128)(2,1)}), bf16[32,8,2048]{2,1,0:T(8,128)(2,1)S(1)}, u32[]{:S(2)}, u32[]{:S(2)}) %all-to-all-start) | async-done | bytes 1048608 | tf_op jit(solution)/shard_map/all_to_all | solution.py:296
  51.3 0.0 collective-permute-done.2.refs_3_
  51.3 1.0 copy-done.3
  52.3 8.4 %shard_map.201 = (bf16[16,128,128]{2,1,0:T(8,128)(2,1)}, bf16[4,256,384]{2,1,0:T(8,128)(2,1)}) custom-call(bf16[256,2048]{1,0:T(8,128)(2,1)} %bitcast.44, bf16[2048,384]{1,0:T(8,128)(2,1)} %shard_map.200.refs_0_, bf16[2048,384]{1,0:T(8,128)(2,1)} %collective-permute-done.refs_1_, bf16[2048,384]{1,0:T(8,128)(2,1)} %collective-permute-done.1.refs_2_, ...), custom_call_target="tpu_custom_call" | custom-call | flops 2147483648 | bytes 1048576 | tf_op jit(solution)/shard_map/pallas_call | solution.py:25
  60.7 0.0 copy-start.13
  60.7 0.0 copy-start.5
  60.7 0.0 copy-start.8
  60.7 0.0 copy-start.12
  60.7 0.0 copy-start.7
  60.7 5.5 %shard_map.202 = (bf16[2,2048,384]{2,1,0:T(8,128)(2,1)}, bf16[2,2048,384]{2,1,0:T(8,128)(2,1)}) custom-call(bf16[256,2048]{1,0:T(8,128)(2,1)} %bitcast.45, bf16[4,256,384]{2,1,0:T(8,128)(2,1)} %get-tuple-element.21.z_ref), custom_call_target="tpu_custom_call" | custom-call | flops 2147483648 | bytes 1048576 | tf_op jit(solution)/shard_map/pallas_call | solution.py:25
  66.2 4.8 %collective-permute-start.3 = (bf16[2,2048,384]{2,1,0:T(8,128)(2,1)}, bf16[2,2048,384]{2,1,0:T(8,128)(2,1)S(1)}, u32[]{:S(2)}, u32[]{:S(2)}) collective-permute-start(bf16[2,2048,384]{2,1,0:T(8,128)(2,1)} %get-tuple-element.23), channel_id=1, source_target_pairs={{0,1},{1,0},{2,3},{3,2},{4,5},{5,4},{6,7},{7,6},{8,9},{9,8},{10,11... | collective-permute-start | bytes 9437192 | tf_op jit(solution)/shard_map/ppermute | solution.py:327
  71.1 0.0 copy-done.5
  71.1 0.0 copy-done.8
  71.1 0.0 copy-done.12
  71.1 0.2 bitcast_dynamic-update-slice_fusion.2
  71.4 16.6 %all-to-all-start.1 = ((bf16[512,4,128]{2,1,0:T(4,128)(2,1)}), bf16[512,4,128]{2,1,0:T(4,128)(2,1)}, u32[]{:S(2)}, u32[]{:S(2)}) async-start(bf16[512,4,128]{2,1,0:T(4,128)(2,1)} %bitcast.46), calls=%async_computation.1 | async-start | bytes 1048576 | tf_op jit(solution)/shard_map/all_to_all | solution.py:317
  88.0 1.4 constant_dynamic-slice_fusion.own_ref
  89.4 0.0 collective-permute-done.3.got_ref
  89.4 1.7 copy-done
  91.1 4.9 %shard_map.203 = (bf16[2048,384]{1,0:T(8,128)(2,1)}, bf16[2048,384]{1,0:T(8,128)(2,1)}) custom-call(bf16[2,2048,384]{2,1,0:T(8,128)(2,1)} %get-tuple-element.22.own_ref, bf16[2,2048,384]{2,1,0:T(8,128)(2,1)} %copy-done), custom_call_target="tpu_custom_call" | custom-call | flops 134217728 | bytes 1048576 | tf_op jit(solution)/shard_map/pallas_call | solution.py:25
  96.0 3.4 %collective-permute-start.4 = (bf16[2048,384]{1,0:T(8,128)(2,1)}, bf16[2048,384]{1,0:T(8,128)(2,1)S(1)}, u32[]{:S(2)}, u32[]{:S(2)}) collective-permute-start(bf16[2048,384]{1,0:T(8,128)(2,1)} %get-tuple-element.25), channel_id=1, source_target_pairs={{0,2},{1,3},{2,0},{3,1},{4,6},{5,7},{6,4},{7,5},{8,10},{9,11},{10,... | collective-permute-start | bytes 4718600 | tf_op jit(solution)/shard_map/ppermute | solution.py:331
  99.5 0.2 fusion.10
  99.7 0.1 bitcast_dynamic-update-slice_fusion.1
  99.8 0.0 copy-start.4
  99.8 8.8 %all-to-all-done.1 = bf16[512,4,128]{2,1,0:T(4,128)(2,1)} async-done(((bf16[512,4,128]{2,1,0:T(4,128)(2,1)}), bf16[512,4,128]{2,1,0:T(4,128)(2,1)}, u32[]{:S(2)}, u32[]{:S(2)}) %all-to-all-start.1) | async-done | bytes 524320 | tf_op jit(solution)/shard_map/all_to_all | solution.py:317
  108.6 2.2 %shard_map.205 = bf16[128,128]{1,0:T(8,128)(2,1)} custom-call(s32[128,2]{1,0:T(8,128)} %copy.22.ids_ref, bf16[2048,128]{1,0:T(8,128)(2,1)} %bitcast.9.recv_ref, bf16[128,128]{1,0:T(8,128)(2,1)} %constant_dynamic-slice_fusion.own_ref), custom_call_target="tpu_custom_call" | custom-call | flops 134217728 | bytes 1048576 | tf_op jit(solution)/shard_map/pallas_call | solution.py:25
  110.8 39.0 %all-gather = bf16[2048,128]{1,0:T(8,128)(2,1)} all-gather(bf16[128,128]{1,0:T(8,128)(2,1)} %shard_map.205), channel_id=2, replica_groups=mesh['sp'=32,'tp'=16] {'tp'}, dimensions={0}, use_global_device_ids=true | all-gather | bytes 557056 | tf_op jit(solution)/shard_map/all_gather | solution.py:335
  149.8 3.1 %shard_map.206 = (bf16[32,24,128]{2,1,0:T(8,128)(2,1)}, f32[32,128]{1,0:T(8,128)}, f32[32,128]{1,0:T(8,128)}, f32[32,128]{1,0:T(8,128)}) custom-call(bf16[16,128,128]{2,1,0:T(8,128)(2,1)} %bitcast.43, bf16[32,2048]{1,0:T(8,128)(2,1)} %bitcast.50, bf16[32,128]{1,0:T(8,128)(2,1)} %mixed_ref.1, f32[6,32,128]{2,1,0:T(8,128)} %copy-done.4), custom_call_target="tpu_custom_call" | custom-call | flops 134217728 | bytes 1048576 | tf_op jit(solution)/shard_map/pallas_call | solution.py:25
  152.8 22.1 %all_to_all.15.recv_ref = bf16[32,24,128]{2,1,0:T(8,128)(2,1)} all-to-all(bf16[32,24,128]{2,1,0:T(8,128)(2,1)} %get-tuple-element.30), channel_id=1, replica_groups=mesh['sp'=32,'tp'=16] {'sp'}, dimensions={0} | all-to-all | bytes 393216 | tf_op jit(solution)/shard_map/all_to_all | solution.py:350
  174.9 2.0 %shard_map.207 = (f32[64,32]{1,0:T(8,128)}, f32[32,128]{1,0:T(8,128)}) custom-call(bf16[32,24,128]{2,1,0:T(8,128)(2,1)} %all_to_all.15.recv_ref, f32[32,128]{1,0:T(8,128)} %get-tuple-element.31.adj_ref, f32[32,128]{1,0:T(8,128)} %get-tuple-element.32.tail_ref, f32[6,32,128]{2,1,0:T(8,128)} %copy-done.4, bf16[32,32]{1,0:T(8,128)(2,1)} %bitcast.51, ...), custom_call_target="tpu_custom_call" | custom-call | flops 33554432 | bytes 1048576 | tf_op jit(solution)/shard_map/pallas_call | solution.py:25
  176.9 1.4 copy.25
  178.4 0.0 collective-permute-done.4.b_ref
  178.4 1.2 copy-done.1
  179.6 3.3 %shard_map.204 = (bf16[2048,128]{1,0:T(8,128)(2,1)}, bf16[2048,128]{1,0:T(8,128)(2,1)}, bf16[128,2048]{1,0:T(8,128)(2,1)}) custom-call(bf16[2048,384]{1,0:T(8,128)(2,1)} %get-tuple-element.24.a_ref, bf16[2048,384]{1,0:T(8,128)(2,1)} %copy-done.1), custom_call_target="tpu_custom_call" | custom-call | flops 134217728 | bytes 1048576 | tf_op jit(solution)/shard_map/pallas_call | solution.py:25
  (17 shorter events, 0.1 us)
Async XLA Ops:
  0.6 6.9 %copy-start.10 = (s32[128,2]{0,1:T(2,128)S(1)}, s32[128,2]{0,1:T(2,128)}, u32[]{:S(2)}) copy-start(s32[128,2]{0,1:T(2,128)} %param.18) | copy-start | bytes 3076
  0.6 7.7 %copy-start.11 = (f32[128,2]{0,1:T(2,128)S(1)}, f32[128,2]{0,1:T(2,128)}, u32[]{:S(2)}) copy-start(f32[128,2]{0,1:T(2,128)} %param.19) | copy-start | bytes 3076
  3.5 33.6 %collective-permute-start.1 = (bf16[2048,384]{1,0:T(8,128)(2,1)}, bf16[2048,384]{1,0:T(8,128)(2,1)}, u32[]{:S(2)}, u32[]{:S(2)}) collective-permute-start(bf16[2048,384]{1,0:T(8,128)(2,1)} %shard_map.200.refs_0_), channel_id=1, source_target_pairs={{0,2},{1,3},{2,0},{3,1},{4,6},{5,7},{6,4},{7,5},{8,10},{9,11},{10,... | collective-permute-start | bytes 4718600 | tf_op jit(solution)/shard_map/ppermute | solution.py:285
  12.3 13.0 %copy-start.2 = (bf16[2048,384]{1,0:T(8,128)(2,1)S(1)}, bf16[2048,384]{1,0:T(8,128)(2,1)}, u32[]{:S(2)}) copy-start(bf16[2048,384]{1,0:T(8,128)(2,1)} %shard_map.200.refs_0_) | copy-start | bytes 4718596
  12.3 39.1 %all-to-all-start = ((bf16[32,8,2048]{2,1,0:T(8,128)(2,1)}), bf16[32,8,2048]{2,1,0:T(8,128)(2,1)S(1)}, u32[]{:S(2)}, u32[]{:S(2)}) async-start(bf16[32,8,2048]{2,1,0:T(8,128)(2,1)} %bitcast.42), calls=%async_computation | async-start | bytes 2097152 | tf_op jit(solution)/shard_map/all_to_all | solution.py:296
  25.3 19.8 %collective-permute-start = (bf16[2048,384]{1,0:T(8,128)(2,1)S(1)}, bf16[2048,384]{1,0:T(8,128)(2,1)}, u32[]{:S(2)}, u32[]{:S(2)}) collective-permute-start(bf16[2048,384]{1,0:T(8,128)(2,1)S(1)} %copy-done.2), channel_id=1, source_target_pairs={{0,1},{1,0},{2,3},{3,2},{4,5},{5,4},{6,7},{7,6},{8,9},{9,8},{10,11... | collective-permute-start | bytes 4718600 | tf_op jit(solution)/shard_map/ppermute | solution.py:286
  37.1 14.2 %collective-permute-start.2 = (bf16[2048,384]{1,0:T(8,128)(2,1)}, bf16[2048,384]{1,0:T(8,128)(2,1)}, u32[]{:S(2)}, u32[]{:S(2)}) collective-permute-start(bf16[2048,384]{1,0:T(8,128)(2,1)} %collective-permute-done.1.refs_2_), channel_id=1, source_target_pairs={{0,1},{1,0},{2,3},{3,2},{4,5},{5,4},{6,7},{7,6},{8,9},{9,8},{10,11... | collective-permute-start | bytes 4718600 | tf_op jit(solution)/shard_map/ppermute | solution.py:298
  51.3 1.0 copy-start.3
  60.7 10.4 %copy-start.13 = (f32[32]{0:T(128)S(1)}, f32[32]{0:T(128)}, u32[]{:S(2)}) copy-start(f32[32]{0:T(128)} %param.30) | copy-start | bytes 388
  60.7 10.4 %copy-start.5 = (bf16[32,128]{1,0:T(8,128)(2,1)S(1)}, bf16[32,128]{1,0:T(8,128)(2,1)}, u32[]{:S(2)}) copy-start(bf16[32,128]{1,0:T(8,128)(2,1)} %param.25) | copy-start | bytes 24580
  60.7 10.4 %copy-start.8 = (bf16[1,32,32]{2,1,0:T(8,128)(2,1)S(1)}, bf16[1,32,32]{2,1,0:T(8,128)(2,1)}, u32[]{:S(2)}) copy-start(bf16[1,32,32]{2,1,0:T(8,128)(2,1)} %param.28) | copy-start | bytes 6148
  60.7 10.4 %copy-start.12 = (f32[32,128]{1,0:T(8,128)S(1)}, f32[32,128]{1,0:T(8,128)}, u32[]{:S(2)}) copy-start(f32[32,128]{1,0:T(8,128)} %param.31) | copy-start | bytes 49156
  60.7 10.6 %copy-start.7 = (bf16[32,128]{1,0:T(8,128)(2,1)S(1)}, bf16[32,128]{1,0:T(8,128)(2,1)}, u32[]{:S(2)}) copy-start(bf16[32,128]{1,0:T(8,128)(2,1)} %param.26) | copy-start | bytes 24580
  66.2 23.2 %collective-permute-start.3 = (bf16[2,2048,384]{2,1,0:T(8,128)(2,1)}, bf16[2,2048,384]{2,1,0:T(8,128)(2,1)S(1)}, u32[]{:S(2)}, u32[]{:S(2)}) collective-permute-start(bf16[2,2048,384]{2,1,0:T(8,128)(2,1)} %get-tuple-element.23), channel_id=1, source_target_pairs={{0,1},{1,0},{2,3},{3,2},{4,5},{5,4},{6,7},{7,6},{8,9},{9,8},{10,11... | collective-permute-start | bytes 9437192 | tf_op jit(solution)/shard_map/ppermute | solution.py:327
  71.4 37.2 %all-to-all-start.1 = ((bf16[512,4,128]{2,1,0:T(4,128)(2,1)}), bf16[512,4,128]{2,1,0:T(4,128)(2,1)}, u32[]{:S(2)}, u32[]{:S(2)}) async-start(bf16[512,4,128]{2,1,0:T(4,128)(2,1)} %bitcast.46), calls=%async_computation.1 | async-start | bytes 1048576 | tf_op jit(solution)/shard_map/all_to_all | solution.py:317
  89.4 1.7 copy-start
  91.1 8.4 %copy-start.6 = (f32[32,128]{1,0:T(8,128)S(1)}, f32[32,128]{1,0:T(8,128)}, u32[]{:S(2)}) copy-start(f32[32,128]{1,0:T(8,128)} %param.27) | copy-start | bytes 49156
  91.1 8.4 %copy-start.9 = (bf16[1,32,32]{2,1,0:T(8,128)(2,1)S(1)}, bf16[1,32,32]{2,1,0:T(8,128)(2,1)}, u32[]{:S(2)}) copy-start(bf16[1,32,32]{2,1,0:T(8,128)(2,1)} %param.29) | copy-start | bytes 6148
  96.0 82.4 %collective-permute-start.4 = (bf16[2048,384]{1,0:T(8,128)(2,1)}, bf16[2048,384]{1,0:T(8,128)(2,1)S(1)}, u32[]{:S(2)}, u32[]{:S(2)}) collective-permute-start(bf16[2048,384]{1,0:T(8,128)(2,1)} %get-tuple-element.25), channel_id=1, source_target_pairs={{0,2},{1,3},{2,0},{3,1},{4,6},{5,7},{6,4},{7,5},{8,10},{9,11},{10,... | collective-permute-start | bytes 4718600 | tf_op jit(solution)/shard_map/ppermute | solution.py:331
  99.8 50.0 %copy-start.4 = (f32[6,32,128]{2,1,0:T(8,128)}, f32[6,32,128]{2,1,0:T(8,128)S(1)}, u32[]{:S(2)}) copy-start(f32[6,32,128]{2,1,0:T(8,128)S(1)} %bitcast_dynamic-update-slice_fusion.fac_ref) | copy-start | bytes 294916
  178.4 1.2 copy-start.1

commit v2 on v1

v2 whole, which is shorter than its diff:
```python
import jax
import jax.numpy as jnp
from jax import lax
from jax.experimental import pallas as pl
from jax.experimental.pallas import tpu as pltpu
from jax.sharding import PartitionSpec as P


RATE_SCALE = 8.0
CLAMP_LIMIT = 7.0
GLU_ALPHA = 1.702
F32 = jnp.float32
BF16 = jnp.bfloat16
SUB = 4
PAIR = 2 * SUB


def dot(a, b, ca=1, cb=0):
    return lax.dot_general(a, b, (((ca,), (cb,)), ((), ())), preferred_element_type=F32)


def call(body, out, *args, flops=0, scratch=(), specs=None, grant=20):
    out = tuple(out) if isinstance(out, (list, tuple)) else out
    return pl.pallas_call(
        body,
        out_shape=out,
        in_specs=specs if specs else [pl.BlockSpec(memory_space=pltpu.VMEM)] * len(args),
        scratch_shapes=list(scratch),
        compiler_params=pltpu.CompilerParams(vmem_limit_bytes=grant << 20),
        cost_estimate=pl.CostEstimate(flops=flops, bytes_accessed=1 << 20, transcendentals=0),
    )(*args)


def sds(shape, dtype):
    return jax.ShapeDtypeStruct(shape, dtype)


def iota(shape, dim):
    return lax.broadcasted_iota(jnp.int32, shape, dim)


def route_body(ids_ref, w_ref, stream_ref, cot_ref, o_ref):
    tok, rows = stream_ref.shape[0], o_ref.shape[0]
    sub = lax.axis_index("y") % 2 * 2 + lax.axis_index("core")
    line = iota((rows, tok), 0)
    expert = line // 8
    slot = line % SUB + sub * SUB
    is_grad = (line % 8) >= SUB

    def along_lanes(ref, k):
        return jnp.broadcast_to(ref[k : k + 1, :], (rows, tok))

    first = along_lanes(ids_ref, 0) == expert
    second = along_lanes(ids_ref, 1) == expert
    named = first | second
    before = dot(
        jnp.where(named, 1.0, 0.0).astype(BF16),
        jnp.where(iota((tok, tok), 0) < iota((tok, tok), 1), 1.0, 0.0).astype(BF16),
    )
    here = named & (before == slot.astype(F32))
    weight = jnp.where(first, along_lanes(w_ref, 0), along_lanes(w_ref, 1))
    weight = jnp.sum(jnp.where(here & is_grad, weight, 0.0), axis=1, keepdims=True)
    weight = jnp.where(is_grad[:, 0:1], weight, 1.0)
    pick_x = jnp.where(here & ~is_grad, 1.0, 0.0).astype(BF16)
    pick_g = jnp.where(here & is_grad, 1.0, 0.0).astype(BF16)
    for j in range(stream_ref.shape[1] // 512):
        cols = slice(512 * j, 512 * (j + 1))
        both = dot(pick_x, stream_ref[:, cols]) + dot(pick_g, cot_ref[:, cols])
        o_ref[:, cols] = (both * weight).astype(BF16)


def expert_body(ra_ref, rb_ref, *refs):
    weights, (keep_ref, swap_ref, z_ref, both, down, rows_ref, sems) = refs[:6], refs[6:]
    part_rows = ra_ref.shape[0]
    rows = 2 * part_rows
    me = lax.axis_index("core")
    copies = []
    for k in range(2):
        places = (both.at[k, :, 0:128], both.at[k, :, 128:256], down.at[k])
        for n, place in enumerate(places):
            copies.append(pltpu.make_async_copy(weights[3 * k + n], place, sems.at[3 * k + n]))
    for copy in copies:
        copy.start()
    rows_ref[0:part_rows] = ra_ref[...]
    rows_ref[part_rows:rows] = rb_ref[...]
    is_x = (iota((rows, 128), 0) % 8) < SUB
    want = iota((part_rows, rows), 0)
    slot = want % PAIR
    source = jnp.where(slot // SUB == me, 0, part_rows) + (want // PAIR) * 8 + slot % SUB
    pick = jnp.where(source == iota((part_rows, rows), 1), 1.0, 0.0).astype(BF16)
    total = None
    for k in range(2):
        copies[3 * k].wait()
        copies[3 * k + 1].wait()
        pre = dot(rows_ref[...], both[k])
        copies[3 * k + 2].wait()
        d_act = pltpu.roll(dot(rows_ref[...], down[k], 1, 1), rows - SUB, 0)
        gate, up = pre[:, 0:128], pre[:, 128:256]
        glu = jnp.minimum(gate, CLAMP_LIMIT)
        lin = jnp.clip(up, -CLAMP_LIMIT, CLAMP_LIMIT) + 1.0
        sig = jax.nn.sigmoid(GLU_ALPHA * glu)
        swish = glu * sig
        act = swish * lin
        slope = lin * (sig + GLU_ALPHA * swish * (1.0 - sig))
        d_gate = jnp.where(is_x & (gate <= CLAMP_LIMIT), d_act * slope, 0.0)
        d_up = jnp.where(is_x & (jnp.abs(up) <= CLAMP_LIMIT), d_act * swish, 0.0)
        act = jnp.where(is_x, 0.0, pltpu.roll(act, SUB, 0))
        d_both = jnp.concatenate([d_gate, d_up], axis=1).astype(BF16)
        z_ref[k, :, 0:256] = d_both
        z_ref[k, :, 256:384] = act.astype(BF16)
        part = dot(dot(pick, d_both).astype(BF16), both[k], 1, 1)
        total = part if total is None else total + part
    for j in range(keep_ref.shape[0]):
        even = total[:, 256 * j : 256 * j + 128].astype(BF16)
        odd = total[:, 256 * j + 128 : 256 * j + 256].astype(BF16)
        keep_ref[j] = jnp.where(me == 0, even, odd)
        swap_ref[j] = jnp.where(me == 0, odd, even)


def grads_of(ra_ref, rb_ref, z_ref, k):
    rows = ra_ref.shape[0]
    return dot(ra_ref[...].T, z_ref[k, 0:rows]) + dot(rb_ref[...].T, z_ref[k, rows : 2 * rows])


def send_body(ra_ref, rb_ref, z_ref, o_ref):
    o_ref[...] = grads_of(ra_ref, rb_ref, z_ref, 1).astype(BF16)


def keep_body(ra_ref, rb_ref, z_ref, got_ref, gate_ref, up_ref, down_ref):
    total = grads_of(ra_ref, rb_ref, z_ref, 0) + got_ref[...].astype(F32)
    gate_ref[...] = total[:, 0:128].astype(BF16)
    up_ref[...] = total[:, 128:256].astype(BF16)
    for j in range(down_ref.shape[1] // 128):
        lines = slice(128 * j, 128 * (j + 1))
        down_ref[:, lines] = total[lines, 256:384].T.astype(BF16)


def places_body(ids_ref, o_ref):
    tok, lanes = o_ref.shape
    col = iota((tok, lanes), 1)
    half = lanes // 2
    slot = (col // half) * PAIR + col % PAIR
    expert = (col % half) // PAIR

    def named_by(k):
        one = jnp.broadcast_to(ids_ref[k : k + 1, :], (tok, tok)).T
        return jnp.concatenate([one] * (lanes // tok), axis=1) == expert

    named = named_by(0) | named_by(1)
    before = dot(
        jnp.where(iota((tok, tok), 0) > iota((tok, tok), 1), 1.0, 0.0).astype(BF16),
        jnp.where(named, 1.0, 0.0).astype(BF16),
    )
    o_ref[...] = jnp.where(named & (before == slot.astype(F32)), 1.0, 0.0).astype(BF16)


def combine_body(pick_ref, recv_ref, own_ref, o_ref):
    lanes = pick_ref.shape[1]
    total = own_ref[...].astype(F32)
    for k in range(recv_ref.shape[0] // lanes):
        total = total + dot(pick_ref[...], recv_ref[lanes * k : lanes * (k + 1)])
    o_ref[...] = total.astype(BF16)


def in_three(x):
    high = x.astype(BF16)
    rest = x - high.astype(F32)
    mid = rest.astype(BF16)
    return high, mid, (rest - mid.astype(F32)).astype(BF16)


def scan_body(s_ref, proj_ref, mixed_ref, fac_ref, pay_ref, gb_ref, adj_ref, tail_ref):
    ch, tok = mixed_ref.shape
    blocks = s_ref.shape[0]
    low = iota((16, 128), 1) < 64
    d_mixed = jnp.zeros((ch, tok), F32)
    for j in range(blocks):
        s = s_ref[j]
        d_mixed = d_mixed + dot(proj_ref[:, 128 * j : 128 * (j + 1)], s, 1, 1)
        g = dot(mixed_ref[...], s)
        a, b = g[0:16], g[16:32]
        pay_ref[2 * j, 0:16] = jnp.where(low, a, pltpu.roll(b, 64, 1)).astype(BF16)
        pay_ref[2 * j + 1, 0:16] = jnp.where(low, pltpu.roll(a, 64, 1), b).astype(BF16)
    decay = fac_ref[0]
    gb_ref[...] = d_mixed * fac_ref[2]
    at = iota((ch, tok), 1)
    val = d_mixed * fac_ref[1]
    mul = jnp.where(at < tok - 1, pltpu.roll(decay, tok - 1, 1), 1.0)
    step = 1
    while step < tok:
        inside = at < tok - step
        later_val = jnp.where(inside, pltpu.roll(val, tok - step, 1), 0.0)
        later_mul = jnp.where(inside, pltpu.roll(mul, tok - step, 1), 1.0)
        val = val + mul * later_val
        mul = mul * later_mul
        step *= 2
    adj_ref[...] = val
    tail_ref[...] = mul
    first = at == 0
    head = jnp.sum(jnp.where(first, decay * val, 0.0), axis=1, keepdims=True)
    prod = jnp.sum(jnp.where(first, decay * mul, 0.0), axis=1, keepdims=True)
    cols = jnp.where(first, prod, jnp.where(at == 1, head, 0.0))
    cols = jnp.concatenate([cols, jnp.zeros((tok - ch, tok), F32)], axis=0)
    lines = cols.T[0:8]
    high, mid, rest = in_three(lines)
    lines = (
        high.astype(F32)
        + pltpu.roll(mid.astype(F32), 32, 1)
        + pltpu.roll(rest.astype(F32), 64, 1)
    ).astype(BF16)
    for k in range(pay_ref.shape[0]):
        pay_ref[k, 16:24] = lines


def finish_body(recv_ref, adj_ref, tail_ref, fac_ref, rg_ref, ig_ref, gp_ref, gr_ref):
    count = recv_ref.shape[0]
    me = lax.axis_index("sp")
    total = recv_ref[0, 0:16].astype(F32)
    for k in range(1, count):
        total = total + recv_ref[k, 0:16].astype(F32)
    gp_ref[0:16] = total[:, 0:64]
    gp_ref[16:32] = total[:, 64:128]
    carried = jnp.zeros((1, 128), F32)
    for k in range(count - 1, -1, -1):
        x = recv_ref[k, 16:24].astype(F32)
        x = x + pltpu.roll(x, 96, 1) + pltpu.roll(x, 64, 1)
        new = x[1:2] + x[0:1] * carried
        carried = jnp.where(k > me, new, carried)
    ch = adj_ref.shape[0]
    carried = jnp.broadcast_to(carried, (128, 128)).T[0:ch]
    adj = adj_ref[...] + tail_ref[...] * carried
    d_rec = (adj * fac_ref[3]).astype(BF16)
    d_in = (adj * fac_ref[4]).astype(BF16)
    gr_ref[...] = adj * fac_ref[5] + dot(rg_ref[...], d_rec) + dot(ig_ref[...], d_in)


def recurrence_factors(rec_input, branch_input, state_before, rec_gates, in_gates, decay_param, decay_shift):
    _, positions = rec_input.shape
    rec_pre = dot(rec_gates, rec_input, 0, 0)
    in_pre = dot(in_gates, rec_input, 0, 0)
    rec_gate = jax.nn.sigmoid(rec_pre)
    in_gate = jax.nn.sigmoid(in_pre)
    soft_plus = jax.nn.softplus(-decay_param)[:, None]
    log_decay = -RATE_SCALE * rec_gate * soft_plus + decay_shift
    decay = jnp.exp(log_decay)
    at_start = (lax.axis_index("sp") * positions + jnp.arange(positions, dtype=jnp.int32) == 0)[None, :]
    raw_mult = jnp.sqrt(-jnp.expm1(2.0 * log_decay))
    multiplier = jnp.where(at_start, 1.0, raw_mult)
    rec_value = rec_input.astype(F32)
    state_now = decay * state_before + multiplier * in_gate * rec_value
    gelu_val, gelu_vjp = jax.vjp(jax.nn.gelu, branch_input.astype(F32))
    branch = gelu_vjp(state_now)[0]
    mult_term = jnp.where(at_start, 0.0, in_gate * rec_value * decay * decay / raw_mult)
    d_log = state_before * decay - mult_term
    d_rec = d_log * (-RATE_SCALE * soft_plus) * rec_gate * (1.0 - rec_gate)
    d_in = multiplier * rec_value * in_gate * (1.0 - in_gate)
    return jnp.stack([decay, gelu_val, branch, d_rec, d_in, multiplier * in_gate])


def local(
    stream,
    cotangent,
    route_ids,
    route_weights,
    w_gate,
    w_up,
    w_down,
    out_proj,
    mixed,
    rec_input,
    branch_input,
    state_before,
    rec_gates,
    in_gates,
    decay_param,
    decay_shift,
):
    sp_count, chips = lax.axis_size("sp"), lax.axis_size("y")
    tok, width = cotangent.shape
    core = [(0, 1), (1, 0)]
    chip = [(i, i ^ 1) for i in range(chips)]

    own = (w_gate[0], w_up[0], w_down[0])
    across = []
    for w in own:
        across.append(lax.ppermute(w, "y", chip))
    ids = route_ids.T
    lines = sp_count * PAIR
    rows = call(
        route_body,
        sds((lines, width), BF16),
        ids,
        route_weights.T,
        stream,
        cotangent,
        flops=1 << 28,
        grant=60,
    )
    mine = lax.all_to_all(rows.reshape(sp_count, 8, width), "sp", 0, 0, tiled=True)
    mine = mine.reshape(lines, width)
    theirs = lax.ppermute(mine, "core", core)
    vmem, hbm = pl.BlockSpec(memory_space=pltpu.VMEM), pl.BlockSpec(memory_space=pl.ANY)

    terms, terms_theirs, z = call(
        expert_body,
        (
            sds((chips, lines, 128), BF16),
            sds((chips, lines, 128), BF16),
            sds((2, 2 * lines, 384), BF16),
        ),
        mine,
        theirs,
        *own,
        *across,
        flops=1 << 31,
        specs=[vmem] * 2 + [hbm] * 6,
        scratch=(
            pltpu.VMEM((2, width, 256), BF16),
            pltpu.VMEM((2, 128, width), BF16),
            pltpu.VMEM((2 * lines, width), BF16),
            pltpu.SemaphoreType.DMA((6,)),
        ),
    )
    terms_got = lax.ppermute(terms_theirs, "core", core)
    grads = call(send_body, sds((width, 384), BF16), mine, theirs, z, flops=1 << 30)
    grads_got = lax.ppermute(grads, "y", chip)
    terms = (terms.astype(F32) + terms_got.astype(F32)).astype(BF16)
    terms = terms.reshape(chips * sp_count, PAIR, 128)
    back = lax.all_to_all(terms, ("y", "sp"), 0, 0, tiled=True)
    back = back.reshape(-1, 128)

    own_cols = lax.dynamic_slice_in_dim(cotangent, lax.axis_index(("y", "core")) * 128, 128, 1)
    pick = call(places_body, sds((tok, 2 * lines), BF16), ids, flops=1 << 25)
    share = call(combine_body, sds((tok, 128), BF16), pick, back, own_cols, flops=1 << 27)
    low = lax.all_gather(share, ("y", "core"), axis=0)
    factors = recurrence_factors(
        rec_input, branch_input, state_before, rec_gates[0], in_gates[0], decay_param, decay_shift
    )
    channels = mixed.shape[0]
    plane = sds((channels, tok), F32)
    payload, grad_branch, adj, tail = call(
        scan_body,
        (sds((sp_count, 24, 128), BF16), plane, plane, plane),
        low,
        out_proj.T,
        mixed,
        factors,
        flops=1 << 27,
    )
    final = lax.all_to_all(payload, "sp", 0, 0, tiled=True)
    grad_proj, grad_rec = call(
        finish_body,
        (sds((channels, width // sp_count), F32), plane),
        final,
        adj,
        tail,
        factors,
        rec_gates[0],
        in_gates[0],
        flops=1 << 25,
    )
    half = sds((width, 128), BF16)
    grad_gate, grad_up, grad_down = call(
        keep_body,
        (half, half, sds((128, width), BF16)),
        mine,
        theirs,
        z,
        grads_got,
        flops=1 << 30,
    )
    return (grad_gate[None], grad_up[None], grad_down[None], grad_proj.T, grad_rec, grad_branch)


def solution(mesh):
    devices = mesh.devices
    finer = jax.sharding.Mesh(
        devices.reshape(devices.shape[0], devices.shape[1] // 2, 2), ("sp", "y", "core")
    )
    placed = (
        P("sp", None),
        P("sp", None),
        P("sp", None),
        P("sp", None),
        P("sp", None, ("y", "core")),
        P("sp", None, ("y", "core")),
        P("sp", ("y", "core"), None),
        P(None, ("y", "core")),
        P(("y", "core"), "sp"),
        P(("y", "core"), "sp"),
        P(("y", "core"), "sp"),
        P(("y", "core"), "sp"),
        P(("y", "core"), None, None),
        P(("y", "core"), None, None),
        P(("y", "core")),
        P(("y", "core"), "sp"),
    )

    return jax.shard_map(
        local,
        mesh=finer,
        in_specs=placed,
        out_specs=(
            P("sp", None, ("y", "core")),
            P("sp", None, ("y", "core")),
            P("sp", ("y", "core"), None),
            P("sp", ("y", "core")),
            P(("y", "core"), "sp"),
            P(("y", "core"), "sp"),
        ),
        check_vma=False,
    )
```

time: 184 us -> 199 us (1.082)
  waiting for transfers between devices: 23.7 us -> 64.2 us
  Pallas kernels: 35.4 us -> 21.3 us
  starting transfers between devices: 53.1 us -> 39.6 us
  other arithmetic: 0.17 us -> 6.22 us
  local copies, waits for them, and re-layouts: 8.17 us -> 4.81 us
  blocking collectives: 61 us -> 58.9 us
  matrix products: 0.38 us -> 2.39 us
    ppermute x5 -> x6, waiting for transfers between devices: 8.7 us -> 29.4 us  [the longest x3 29.4 us: local(): across.append(lax.ppermute(w, 'y', chip))]
    all_gather x1, blocking collectives: 39 us -> 18.9 us  [local(): low = lax.all_gather(share, ('y', 'core'), axis=0)]
    all_to_all x2, waiting for transfers between devices: 15 us -> 34.8 us  [the longest x1 28.1 us: local(): back = lax.all_to_all(terms, ('y', 'sp'), 0, 0, tiled=True)]
    all_to_all x1, blocking collectives: 22.1 us -> 40 us  [local(): lax.all_to_all(rows.reshape(sp_count, 8, width), 'sp', 0, 0, tiled=True)]
    pallas_call x9 -> x8, Pallas kernels: 35.4 us -> 21.3 us  [call(): pl.pallas_call(body, out_shape=out, in_specs=specs if specs else [pl.Bloc...]
    all_to_all x2, starting transfers between devices: 29.7 us -> 20.4 us  [the longest x1 14 us: local(): back = lax.all_to_all(terms, ('y', 'sp'), 0, 0, tiled=True)]
    ppermute x5 -> x6, starting transfers between devices: 23.4 us -> 19.2 us  [the longest x3 8.49 us: local(): across.append(lax.ppermute(w, 'y', chip))]
    unnamed x31 -> x28, local copies, waits for them, and re-layouts: 6.8 us -> 3.43 us
  transfers between devices with their start and end apart: 7 -> 8, of which waited for: 3 -> 5; matrix products, arithmetic and copies ran while one was open for 3% -> 5% of each run, Pallas kernels for 8% -> 5%
where the time goes in v2:
time: 199 us; the launch traced here: 198 us
  waiting for transfers between devices  64.2 us (32%)
  blocking collectives  58.9 us (30%)
  starting transfers between devices  39.6 us (20%)
  Pallas kernels  21.3 us (11%)
  other arithmetic  6.22 us (3%)
  local copies, waits for them, and re-layouts  4.81 us (2%)
  matrix products  2.39 us (1%)
    all_to_all x1, blocking collectives, local(): lax.all_to_all(rows.reshape(sp_count, 8, width), 'sp', 0, 0, tiled=True)  40 us
    ppermute x3, waiting for transfers between devices, local(): across.append(lax.ppermute(w, 'y', chip))  29.4 us
    all_to_all x1, waiting for transfers between devices, local(): back = lax.all_to_all(terms, ('y', 'sp'), 0, 0, tiled=True)  28.1 us
    pallas_call x8, Pallas kernels, call(): pl.pallas_call(body, out_shape=out, in_specs=specs if specs else [pl.Bloc...  21.3 us
    all_gather x1, blocking collectives, local(): low = lax.all_gather(share, ('y', 'core'), axis=0)  18.9 us
    all_to_all x1, starting transfers between devices, local(): back = lax.all_to_all(terms, ('y', 'sp'), 0, 0, tiled=True)  14 us
    ppermute x3, starting transfers between devices, local(): across.append(lax.ppermute(w, 'y', chip))  8.49 us
    all_to_all x1, waiting for transfers between devices, local(): final = lax.all_to_all(payload, 'sp', 0, 0, tiled=True)  6.75 us
  transfers between devices with their start and end apart: 8, of which 5 were waited for; matrix products, arithmetic and copies ran while one was open for 5% of the time, Pallas kernels for 5%

profile of v2, /device:TPU:1, one launch (start us, length us, event | category | flops | bytes accessed | tf_op | source)
XLA Modules:
  0.0 198.3 jit_solution(15827331798503286407)
XLA Ops:
  0.6 3.1 %shard_map.199 = bf16[256,2048]{1,0:T(8,128)(2,1)} custom-call(s32[2,128]{1,0:T(2,128)} %bitcast.54, f32[2,128]{1,0:T(2,128)} %bitcast.62, bf16[128,2048]{1,0:T(8,128)(2,1)} %stream_ref.1, bf16[128,2048]{1,0:T(8,128)(2,1)} %cot_ref.1), custom_call_target="tpu_custom_call" | custom-call | flops 268435456 | bytes 1048576 | tf_op jit(solution)/shard_map/pallas_call | solution.py:24
  3.7 40.0 %all_to_all.15 = bf16[32,8,2048]{2,1,0:T(8,128)(2,1)S(1)} all-to-all(bf16[32,8,2048]{2,1,0:T(8,128)(2,1)} %bitcast.60), channel_id=1, replica_groups=mesh['sp'=32,'y'=8,'core'=2] {'sp'}, dimensions={0} | all-to-all | bytes 2097152 | tf_op jit(solution)/shard_map/all_to_all | solution.py:299
  43.7 4.7 %collective-permute-start = (bf16[256,2048]{1,0:T(8,128)(2,1)S(1)}, bf16[256,2048]{1,0:T(8,128)(2,1)S(1)}, u32[]{:S(2)}, u32[]{:S(2)}) collective-permute-start(bf16[256,2048]{1,0:T(8,128)(2,1)S(1)} %bitcast.45), channel_id=1, source_target_pairs={{0,1},{1,0},{2,3},{3,2},{4,5},{5,4},{6,7},{7,6},{8,9},{9,8},{10,11... | collective-permute-start | bytes 3145736 | tf_op jit(solution)/shard_map/ppermute | solution.py:301
  48.4 0.0 copy-done.6
  48.5 3.2 %collective-permute-start.1 = (bf16[2048,128]{1,0:T(8,128)(2,1)S(1)}, bf16[2048,128]{1,0:T(8,128)(2,1)}, u32[]{:S(2)}, u32[]{:S(2)}) collective-permute-start(bf16[2048,128]{1,0:T(8,128)(2,1)S(1)} %bitcast.56), channel_id=1, source_target_pairs={{0,2},{2,0},{4,6},{6,4},{8,10},{10,8},{12,14},{14,12},{1,3},{3,1},... | collective-permute-start | bytes 1572872 | tf_op jit(solution)/shard_map/ppermute | solution.py:286
  51.7 0.0 copy-done.7
  51.7 2.1 %collective-permute-start.2 = (bf16[2048,128]{1,0:T(8,128)(2,1)S(1)}, bf16[2048,128]{1,0:T(8,128)(2,1)}, u32[]{:S(2)}, u32[]{:S(2)}) collective-permute-start(bf16[2048,128]{1,0:T(8,128)(2,1)S(1)} %bitcast.58), channel_id=1, source_target_pairs={{0,2},{2,0},{4,6},{6,4},{8,10},{10,8},{12,14},{14,12},{1,3},{3,1},... | collective-permute-start | bytes 1572872 | tf_op jit(solution)/shard_map/ppermute | solution.py:286
  53.8 3.2 %collective-permute-start.3 = (bf16[128,2048]{1,0:T(8,128)(2,1)}, bf16[128,2048]{1,0:T(8,128)(2,1)}, u32[]{:S(2)}, u32[]{:S(2)}) collective-permute-start(bf16[128,2048]{1,0:T(8,128)(2,1)} %bitcast.6.refs_2_), channel_id=1, source_target_pairs={{0,2},{2,0},{4,6},{6,4},{8,10},{10,8},{12,14},{14,12},{1,3},{3,1},... | collective-permute-start | bytes 1572872 | tf_op jit(solution)/shard_map/ppermute | solution.py:286
  57.0 0.0 copy-done.13
  57.0 0.0 copy-start.11
  57.0 0.0 copy-start.3
  57.0 6.9 %collective-permute-done.1.refs_3_ = bf16[2048,128]{1,0:T(8,128)(2,1)} collective-permute-done((bf16[2048,128]{1,0:T(8,128)(2,1)S(1)}, bf16[2048,128]{1,0:T(8,128)(2,1)}, u32[]{:S(2)}, u32[]{:S(2)}) %collective-permute-start.1) | collective-permute-done | bytes 524320 | tf_op jit(solution)/shard_map/ppermute | solution.py:286
  63.9 11.2 %collective-permute-done.2.refs_4_ = bf16[2048,128]{1,0:T(8,128)(2,1)} collective-permute-done((bf16[2048,128]{1,0:T(8,128)(2,1)S(1)}, bf16[2048,128]{1,0:T(8,128)(2,1)}, u32[]{:S(2)}, u32[]{:S(2)}) %collective-permute-start.2) | collective-permute-done | bytes 524320 | tf_op jit(solution)/shard_map/ppermute | solution.py:286
  75.2 11.2 %collective-permute-done.3.refs_5_ = bf16[128,2048]{1,0:T(8,128)(2,1)} collective-permute-done((bf16[128,2048]{1,0:T(8,128)(2,1)}, bf16[128,2048]{1,0:T(8,128)(2,1)}, u32[]{:S(2)}, u32[]{:S(2)}) %collective-permute-start.3) | collective-permute-done | bytes 524320 | tf_op jit(solution)/shard_map/ppermute | solution.py:286
  86.4 0.0 collective-permute-done.rb_ref
  86.4 1.0 copy-done.8
  87.4 6.7 %shard_map.200 = (bf16[8,256,128]{2,1,0:T(8,128)(2,1)S(1)}, bf16[8,256,128]{2,1,0:T(8,128)(2,1)S(1)}, bf16[2,512,384]{2,1,0:T(8,128)(2,1)S(1)}) custom-call(bf16[256,2048]{1,0:T(8,128)(2,1)S(1)} %bitcast.46, bf16[256,2048]{1,0:T(8,128)(2,1)S(1)} %collective-permute-done.rb_ref, bf16[2048,128]{1,0:T(8,128)(2,1)S(1)} %bitcast.57, ...), custom_call_target="tpu_custom_call" | custom-call | flops 2147483648 | bytes 1048576 | tf_op jit(solution)/shard_map/pallas_call | solution.py:24
  94.1 2.8 %collective-permute-start.5 = (bf16[8,256,128]{2,1,0:T(8,128)(2,1)S(1)}, bf16[8,256,128]{2,1,0:T(8,128)(2,1)S(1)}, u32[]{:S(2)}, u32[]{:S(2)}) collective-permute-start(bf16[8,256,128]{2,1,0:T(8,128)(2,1)S(1)} %get-tuple-element.23), channel_id=1, source_target_pairs={{0,1},{1,0},{2,3},{3,2},{4,5},{5,4},{6,7},{7,6},{8,9},{9,8},{10,11... | collective-permute-start | bytes 1572872 | tf_op jit(solution)/shard_map/ppermute | solution.py:324
  96.9 0.0 copy-done.11
  96.9 0.0 copy-done.3
  96.9 0.0 copy-done.9
  96.9 0.8 bitcast_dynamic-update-slice_fusion.2
  97.8 0.6 fusion.26
  98.4 2.5 %shard_map.201 = bf16[2048,384]{1,0:T(8,128)(2,1)} custom-call(bf16[256,2048]{1,0:T(8,128)(2,1)S(1)} %bitcast.47, bf16[256,2048]{1,0:T(8,128)(2,1)S(1)} %collective-permute-done.rb_ref, bf16[2,512,384]{2,1,0:T(8,128)(2,1)S(1)} %get-tuple-element.18.z_ref), custom_call_target="tpu_custom_call" | custom-call | flops 1073741824 | bytes 1048576 | tf_op jit(solution)/shard_map/pallas_call | solution.py:24
  100.8 3.2 %collective-permute-start.4 = (bf16[2048,384]{1,0:T(8,128)(2,1)}, bf16[2048,384]{1,0:T(8,128)(2,1)}, u32[]{:S(2)}, u32[]{:S(2)}) collective-permute-start(bf16[2048,384]{1,0:T(8,128)(2,1)} %shard_map.201), channel_id=1, source_target_pairs={{0,2},{2,0},{4,6},{6,4},{8,10},{10,8},{12,14},{14,12},{1,3},{3,1},... | collective-permute-start | bytes 4718600 | tf_op jit(solution)/shard_map/ppermute | solution.py:326
  104.0 0.0 collective-permute-done.5
  104.1 0.9 add_convert_fusion
  105.0 14.0 %all-to-all-start.1 = ((bf16[256,8,128]{2,1,0:T(8,128)(2,1)}), bf16[256,8,128]{2,1,0:T(8,128)(2,1)S(1)}, u32[]{:S(2)}, u32[]{:S(2)}) async-start(bf16[256,8,128]{2,1,0:T(8,128)(2,1)} %bitcast.61), calls=%async_computation.1 | async-start | bytes 1048576 | tf_op jit(solution)/shard_map/all_to_all | solution.py:329
  119.0 0.5 add_compare_fusion
  119.6 0.7 copy-done.5
  120.2 0.3 shard_map.203.pick_ref
  120.5 1.4 constant_dynamic-slice_fusion.own_ref
  121.9 1.6 fusion.10
  123.5 1.4 bitcast_dynamic-update-slice_fusion.1
  124.9 1.3 fusion.15
  126.3 1.4 bitcast_dynamic-update-slice_fusion.fac_ref
  127.6 28.1 %all-to-all-done.1 = bf16[256,8,128]{2,1,0:T(8,128)(2,1)S(1)} async-done(((bf16[256,8,128]{2,1,0:T(8,128)(2,1)}), bf16[256,8,128]{2,1,0:T(8,128)(2,1)S(1)}, u32[]{:S(2)}, u32[]{:S(2)}) %all-to-all-start.1) | async-done | bytes 524320 | tf_op jit(solution)/shard_map/all_to_all | solution.py:329
  155.7 0.8 copy-done
  156.5 0.3 shard_map.204
  156.8 18.9 %all-gather = bf16[2048,128]{1,0:T(8,128)(2,1)S(1)} all-gather(bf16[128,128]{1,0:T(8,128)(2,1)S(1)} %shard_map.204), channel_id=2, replica_groups=mesh['sp'=32,'y'=8,'core'=2] {'y','core'}, dimensions={0}, use_global_device_ids=true | all-gather | bytes 557056 | tf_op jit(solution)/shard_map/all_gather | solution.py:335
  175.6 0.9 copy-done.1
  176.5 2.8 %shard_map.205 = (bf16[32,24,128]{2,1,0:T(8,128)(2,1)}, f32[32,128]{1,0:T(8,128)}, f32[32,128]{1,0:T(8,128)S(1)}, f32[32,128]{1,0:T(8,128)S(1)}) custom-call(bf16[16,128,128]{2,1,0:T(8,128)(2,1)S(1)} %bitcast.50, bf16[32,2048]{1,0:T(8,128)(2,1)S(1)} %bitcast.51, bf16[32,128]{1,0:T(8,128)(2,1)S(1)} %copy-done.2, ...), custom_call_target="tpu_custom_call" | custom-call | flops 134217728 | bytes 1048576 | tf_op jit(solution)/shard_map/pallas_call | solution.py:24
  179.3 6.4 %all-to-all-start.2 = ((bf16[32,24,128]{2,1,0:T(8,128)(2,1)}), bf16[32,24,128]{2,1,0:T(8,128)(2,1)S(1)}, u32[]{:S(2)}, u32[]{:S(2)}) async-start(bf16[32,24,128]{2,1,0:T(8,128)(2,1)} %get-tuple-element.24), calls=%async_computation.2 | async-start | bytes 393216 | tf_op jit(solution)/shard_map/all_to_all | solution.py:350
  185.7 0.0 copy-start.4
  185.8 0.0 collective-permute-done.4.got_ref
  185.8 3.9 %shard_map.202 = (bf16[2048,128]{1,0:T(8,128)(2,1)}, bf16[2048,128]{1,0:T(8,128)(2,1)}, bf16[128,2048]{1,0:T(8,128)(2,1)}) custom-call(bf16[256,2048]{1,0:T(8,128)(2,1)S(1)} %bitcast.48, bf16[256,2048]{1,0:T(8,128)(2,1)S(1)} %collective-permute-done.rb_ref, bf16[2,512,384]{2,1,0:T(8,128)(2,1)S(1)} %get-tuple-element.18.z_ref, ...), custom_call_target="tpu_custom_call" | custom-call | flops 1073741824 | bytes 1048576 | tf_op jit(solution)/shard_map/pallas_call | solution.py:24
  189.6 6.8 %all-to-all-done.2.recv_ref = bf16[32,24,128]{2,1,0:T(8,128)(2,1)S(1)} async-done(((bf16[32,24,128]{2,1,0:T(8,128)(2,1)}), bf16[32,24,128]{2,1,0:T(8,128)(2,1)S(1)}, u32[]{:S(2)}, u32[]{:S(2)}) %all-to-all-start.2) | async-done | bytes 196640 | tf_op jit(solution)/shard_map/all_to_all | solution.py:350
  196.4 1.9 shard_map.206
  (16 shorter events, 0.0 us)
Async XLA Ops:
  3.7 44.8 %copy-start.6 = (bf16[1,2048,128]{2,1,0:T(8,128)(2,1)S(1)}, bf16[1,2048,128]{2,1,0:T(8,128)(2,1)}, u32[]{:S(2)}) copy-start(bf16[1,2048,128]{2,1,0:T(8,128)(2,1)} %param.20) | copy-start | bytes 1572868
  3.7 48.0 %copy-start.7 = (bf16[1,2048,128]{2,1,0:T(8,128)(2,1)S(1)}, bf16[1,2048,128]{2,1,0:T(8,128)(2,1)}, u32[]{:S(2)}) copy-start(bf16[1,2048,128]{2,1,0:T(8,128)(2,1)} %param.21) | copy-start | bytes 1572868
  3.7 53.3 %copy-start.13 = (f32[32]{0:T(128)S(1)}, f32[32]{0:T(128)}, u32[]{:S(2)}) copy-start(f32[32]{0:T(128)} %param.30) | copy-start | bytes 388
  43.7 42.7 %collective-permute-start = (bf16[256,2048]{1,0:T(8,128)(2,1)S(1)}, bf16[256,2048]{1,0:T(8,128)(2,1)S(1)}, u32[]{:S(2)}, u32[]{:S(2)}) collective-permute-start(bf16[256,2048]{1,0:T(8,128)(2,1)S(1)} %bitcast.45), channel_id=1, source_target_pairs={{0,1},{1,0},{2,3},{3,2},{4,5},{5,4},{6,7},{7,6},{8,9},{9,8},{10,11... | collective-permute-start | bytes 3145736 | tf_op jit(solution)/shard_map/ppermute | solution.py:301
  48.5 15.5 %collective-permute-start.1 = (bf16[2048,128]{1,0:T(8,128)(2,1)S(1)}, bf16[2048,128]{1,0:T(8,128)(2,1)}, u32[]{:S(2)}, u32[]{:S(2)}) collective-permute-start(bf16[2048,128]{1,0:T(8,128)(2,1)S(1)} %bitcast.56), channel_id=1, source_target_pairs={{0,2},{2,0},{4,6},{6,4},{8,10},{10,8},{12,14},{14,12},{1,3},{3,1},... | collective-permute-start | bytes 1572872 | tf_op jit(solution)/shard_map/ppermute | solution.py:286
  51.7 23.5 %collective-permute-start.2 = (bf16[2048,128]{1,0:T(8,128)(2,1)S(1)}, bf16[2048,128]{1,0:T(8,128)(2,1)}, u32[]{:S(2)}, u32[]{:S(2)}) collective-permute-start(bf16[2048,128]{1,0:T(8,128)(2,1)S(1)} %bitcast.58), channel_id=1, source_target_pairs={{0,2},{2,0},{4,6},{6,4},{8,10},{10,8},{12,14},{14,12},{1,3},{3,1},... | collective-permute-start | bytes 1572872 | tf_op jit(solution)/shard_map/ppermute | solution.py:286
  53.8 32.6 %collective-permute-start.3 = (bf16[128,2048]{1,0:T(8,128)(2,1)}, bf16[128,2048]{1,0:T(8,128)(2,1)}, u32[]{:S(2)}, u32[]{:S(2)}) collective-permute-start(bf16[128,2048]{1,0:T(8,128)(2,1)} %bitcast.6.refs_2_), channel_id=1, source_target_pairs={{0,2},{2,0},{4,6},{6,4},{8,10},{10,8},{12,14},{14,12},{1,3},{3,1},... | collective-permute-start | bytes 1572872 | tf_op jit(solution)/shard_map/ppermute | solution.py:286
  57.0 39.9 %copy-start.11 = (f32[32]{0:T(128)}, f32[32]{0:T(128)S(1)}, u32[]{:S(2)}) copy-start(f32[32]{0:T(128)S(1)} %fusion.29) | copy-start | bytes 388
  57.0 39.9 %copy-start.3 = (bf16[1,32,32]{2,1,0:T(8,128)(2,1)S(1)}, bf16[1,32,32]{2,1,0:T(8,128)(2,1)}, u32[]{:S(2)}) copy-start(bf16[1,32,32]{2,1,0:T(8,128)(2,1)} %param.28) | copy-start | bytes 6148
  86.4 1.0 copy-start.8
  87.4 9.5 %copy-start.9 = (bf16[32,128]{1,0:T(8,128)(2,1)S(1)}, bf16[32,128]{1,0:T(8,128)(2,1)}, u32[]{:S(2)}) copy-start(bf16[32,128]{1,0:T(8,128)(2,1)} %param.25) | copy-start | bytes 24580
  87.4 9.5 %copy-start.12 = (f32[32,128]{1,0:T(8,128)S(1)}, f32[32,128]{1,0:T(8,128)}, u32[]{:S(2)}) copy-start(f32[32,128]{1,0:T(8,128)} %param.31) | copy-start | bytes 49156
  87.4 10.3 %copy-start.10 = (bf16[32,128]{1,0:T(8,128)(2,1)S(1)}, bf16[32,128]{1,0:T(8,128)(2,1)}, u32[]{:S(2)}) copy-start(bf16[32,128]{1,0:T(8,128)(2,1)} %param.26) | copy-start | bytes 24580
  94.1 9.9 %collective-permute-start.5 = (bf16[8,256,128]{2,1,0:T(8,128)(2,1)S(1)}, bf16[8,256,128]{2,1,0:T(8,128)(2,1)S(1)}, u32[]{:S(2)}, u32[]{:S(2)}) collective-permute-start(bf16[8,256,128]{2,1,0:T(8,128)(2,1)S(1)} %get-tuple-element.23), channel_id=1, source_target_pairs={{0,1},{1,0},{2,3},{3,2},{4,5},{5,4},{6,7},{7,6},{8,9},{9,8},{10,11... | collective-permute-start | bytes 1572872 | tf_op jit(solution)/shard_map/ppermute | solution.py:324
  100.8 84.9 %collective-permute-start.4 = (bf16[2048,384]{1,0:T(8,128)(2,1)}, bf16[2048,384]{1,0:T(8,128)(2,1)}, u32[]{:S(2)}, u32[]{:S(2)}) collective-permute-start(bf16[2048,384]{1,0:T(8,128)(2,1)} %shard_map.201), channel_id=1, source_target_pairs={{0,2},{2,0},{4,6},{6,4},{8,10},{10,8},{12,14},{14,12},{1,3},{3,1},... | collective-permute-start | bytes 4718600 | tf_op jit(solution)/shard_map/ppermute | solution.py:326
  105.0 70.6 %copy-start.2 = (bf16[32,128]{1,0:T(8,128)(2,1)S(1)}, bf16[32,128]{1,0:T(8,128)(2,1)}, u32[]{:S(2)}) copy-start(bf16[32,128]{1,0:T(8,128)(2,1)} %mixed_ref.1) | copy-start | bytes 24580
  105.0 50.7 %all-to-all-start.1 = ((bf16[256,8,128]{2,1,0:T(8,128)(2,1)}), bf16[256,8,128]{2,1,0:T(8,128)(2,1)S(1)}, u32[]{:S(2)}, u32[]{:S(2)}) async-start(bf16[256,8,128]{2,1,0:T(8,128)(2,1)} %bitcast.61), calls=%async_computation.1 | async-start | bytes 1048576 | tf_op jit(solution)/shard_map/all_to_all | solution.py:329
  119.6 0.7 copy-start.5
  155.7 0.8 copy-start
  175.6 0.9 copy-start.1
  179.3 17.0 %all-to-all-start.2 = ((bf16[32,24,128]{2,1,0:T(8,128)(2,1)}), bf16[32,24,128]{2,1,0:T(8,128)(2,1)S(1)}, u32[]{:S(2)}, u32[]{:S(2)}) async-start(bf16[32,24,128]{2,1,0:T(8,128)(2,1)} %get-tuple-element.24), calls=%async_computation.2 | async-start | bytes 393216 | tf_op jit(solution)/shard_map/all_to_all | solution.py:350
  185.7 10.6 %copy-start.4 = (bf16[1,32,32]{2,1,0:T(8,128)(2,1)S(1)}, bf16[1,32,32]{2,1,0:T(8,128)(2,1)}, u32[]{:S(2)}) copy-start(bf16[1,32,32]{2,1,0:T(8,128)(2,1)} %param.29) | copy-start | bytes 6148

commit v3 on v2

--- a/solution.py
+++ b/solution.py
@@ -69,46 +69,57 @@
         o_ref[:, cols] = (both * weight).astype(BF16)
 
 
-def expert_body(ra_ref, rb_ref, *refs):
-    weights, (keep_ref, swap_ref, z_ref, both, down, rows_ref, sems) = refs[:6], refs[6:]
-    part_rows = ra_ref.shape[0]
-    rows = 2 * part_rows
-    me = lax.axis_index("core")
+def expert_math(rows, both, down):
+    count = rows.shape[0]
+    is_x = (iota((count, 128), 0) % 8) < SUB
+    pre = dot(rows, both)
+    d_act = pltpu.roll(dot(rows, down, 1, 1), count - SUB, 0)
+    gate, up = pre[:, 0:128], pre[:, 128:256]
+    glu = jnp.minimum(gate, CLAMP_LIMIT)
+    lin = jnp.clip(up, -CLAMP_LIMIT, CLAMP_LIMIT) + 1.0
+    sig = jax.nn.sigmoid(GLU_ALPHA * glu)
+    swish = glu * sig
+    act = swish * lin
+    slope = lin * (sig + GLU_ALPHA * swish * (1.0 - sig))
+    d_gate = jnp.where(is_x & (gate <= CLAMP_LIMIT), d_act * slope, 0.0)
+    d_up = jnp.where(is_x & (jnp.abs(up) <= CLAMP_LIMIT), d_act * swish, 0.0)
+    act = jnp.where(is_x, 0.0, pltpu.roll(act, SUB, 0)).astype(BF16)
+    return jnp.concatenate([d_gate, d_up], axis=1).astype(BF16), act
+
+
+def fetch(weights, both, down, sems):
     copies = []
-    for k in range(2):
+    for k in range(len(weights) // 3):
         places = (both.at[k, :, 0:128], both.at[k, :, 128:256], down.at[k])
         for n, place in enumerate(places):
             copies.append(pltpu.make_async_copy(weights[3 * k + n], place, sems.at[3 * k + n]))
     for copy in copies:
         copy.start()
-    rows_ref[0:part_rows] = ra_ref[...]
-    rows_ref[part_rows:rows] = rb_ref[...]
-    is_x = (iota((rows, 128), 0) % 8) < SUB
-    want = iota((part_rows, rows), 0)
+    return copies
+
+
+def expert_body(ra_ref, rb_ref, *refs):
+    weights, (keep_ref, swap_ref, z_ref, both, down, sems) = refs[:6], refs[6:]
+    rows = ra_ref.shape[0]
+    me = lax.axis_index("core")
+    copies = fetch(weights, both, down, sems)
+    want = iota((rows, rows), 0)
     slot = want % PAIR
-    source = jnp.where(slot // SUB == me, 0, part_rows) + (want // PAIR) * 8 + slot % SUB
-    pick = jnp.where(source == iota((part_rows, rows), 1), 1.0, 0.0).astype(BF16)
+    source = (want // PAIR) * 8 + slot % SUB == iota((rows, rows), 1)
     total = None
     for k in range(2):
-        copies[3 * k].wait()
-        copies[3 * k + 1].wait()
-        pre = dot(rows_ref[...], both[k])
-        copies[3 * k + 2].wait()
-        d_act = pltpu.roll(dot(rows_ref[...], down[k], 1, 1), rows - SUB, 0)
-        gate, up = pre[:, 0:128], pre[:, 128:256]
-        glu = jnp.minimum(gate, CLAMP_LIMIT)
-        lin = jnp.clip(up, -CLAMP_LIMIT, CLAMP_LIMIT) + 1.0
-        sig = jax.nn.sigmoid(GLU_ALPHA * glu)
-        swish = glu * sig
-        act = swish * lin
-        slope = lin * (sig + GLU_ALPHA * swish * (1.0 - sig))
-        d_gate = jnp.where(is_x & (gate <= CLAMP_LIMIT), d_act * slope, 0.0)
-        d_up = jnp.where(is_x & (jnp.abs(up) <= CLAMP_LIMIT), d_act * swish, 0.0)
-        act = jnp.where(is_x, 0.0, pltpu.roll(act, SUB, 0))
-        d_both = jnp.concatenate([d_gate, d_up], axis=1).astype(BF16)
-        z_ref[k, :, 0:256] = d_both
-        z_ref[k, :, 256:384] = act.astype(BF16)
-        part = dot(dot(pick, d_both).astype(BF16), both[k], 1, 1)
+        for copy in copies[3 * k : 3 * k + 3]:
+            copy.wait()
+        moved = None
+        for n, ref in enumerate((ra_ref, rb_ref)):
+            d_both, act = expert_math(ref[...], both[k], down[k])
+            if k == 0:
+                z_ref[n, :, 0:256] = d_both
+                z_ref[n, :, 256:384] = act
+            own = slot // SUB == (me if n == 0 else 1 - me)
+            part = dot(jnp.where(source & own, 1.0, 0.0).astype(BF16), d_both)
+            moved = part if moved is None else moved + part
+        part = dot(moved.astype(BF16), both[k], 1, 1)
         total = part if total is None else total + part
     for j in range(keep_ref.shape[0]):
         even = total[:, 256 * j : 256 * j + 128].astype(BF16)
@@ -117,17 +128,19 @@
         swap_ref[j] = jnp.where(me == 0, odd, even)
 
 
-def grads_of(ra_ref, rb_ref, z_ref, k):
-    rows = ra_ref.shape[0]
-    return dot(ra_ref[...].T, z_ref[k, 0:rows]) + dot(rb_ref[...].T, z_ref[k, rows : 2 * rows])
-
-
-def send_body(ra_ref, rb_ref, z_ref, o_ref):
-    o_ref[...] = grads_of(ra_ref, rb_ref, z_ref, 1).astype(BF16)
-
-
-def keep_body(ra_ref, rb_ref, z_ref, got_ref, gate_ref, up_ref, down_ref):
-    total = grads_of(ra_ref, rb_ref, z_ref, 0) + got_ref[...].astype(F32)
+def grads_body(ra_ref, rb_ref, rc_ref, rd_ref, z_ref, *refs):
+    weights, (gate_ref, up_ref, down_ref, both, down, sems) = refs[:3], refs[3:]
+    copies = fetch(weights, both, down, sems)
+    total = None
+    for n, ref in enumerate((ra_ref, rb_ref)):
+        part = dot(ref[...].T, z_ref[n])
+        total = part if total is None else total + part
+    for copy in copies:
+        copy.wait()
+    for ref in (rc_ref, rd_ref):
+        rows = ref[...]
+        z = jnp.concatenate(expert_math(rows, both[0], down[0]), axis=1)
+        total = total + dot(rows.T, z)
     gate_ref[...] = total[:, 0:128].astype(BF16)
     up_ref[...] = total[:, 128:256].astype(BF16)
     for j in range(down_ref.shape[1] // 128):
@@ -299,6 +312,8 @@
     mine = lax.all_to_all(rows.reshape(sp_count, 8, width), "sp", 0, 0, tiled=True)
     mine = mine.reshape(lines, width)
     theirs = lax.ppermute(mine, "core", core)
+    across_mine = lax.ppermute(mine, "y", chip)
+    across_theirs = lax.ppermute(across_mine, "core", core)
     vmem, hbm = pl.BlockSpec(memory_space=pltpu.VMEM), pl.BlockSpec(memory_space=pl.ANY)
 
     terms, terms_theirs, z = call(
@@ -306,7 +321,7 @@
         (
             sds((chips, lines, 128), BF16),
             sds((chips, lines, 128), BF16),
-            sds((2, 2 * lines, 384), BF16),
+            sds((2, lines, 384), BF16),
         ),
         mine,
         theirs,
@@ -317,13 +332,10 @@
         scratch=(
             pltpu.VMEM((2, width, 256), BF16),
             pltpu.VMEM((2, 128, width), BF16),
-            pltpu.VMEM((2 * lines, width), BF16),
             pltpu.SemaphoreType.DMA((6,)),
         ),
     )
     terms_got = lax.ppermute(terms_theirs, "core", core)
-    grads = call(send_body, sds((width, 384), BF16), mine, theirs, z, flops=1 << 30)
-    grads_got = lax.ppermute(grads, "y", chip)
     terms = (terms.astype(F32) + terms_got.astype(F32)).astype(BF16)
     terms = terms.reshape(chips * sp_count, PAIR, 128)
     back = lax.all_to_all(terms, ("y", "sp"), 0, 0, tiled=True)
@@ -361,13 +373,21 @@
     )
     half = sds((width, 128), BF16)
     grad_gate, grad_up, grad_down = call(
-        keep_body,
+        grads_body,
         (half, half, sds((128, width), BF16)),
         mine,
         theirs,
+        across_mine,
+        across_theirs,
         z,
-        grads_got,
-        flops=1 << 30,
+        *own,
+        flops=1 << 31,
+        specs=[vmem] * 5 + [hbm] * 3,
+        scratch=(
+            pltpu.VMEM((1, width, 256), BF16),
+            pltpu.VMEM((1, 128, width), BF16),
+            pltpu.SemaphoreType.DMA((3,)),
+        ),
     )
     return (grad_gate[None], grad_up[None], grad_down[None], grad_proj.T, grad_rec, grad_branch)
 

time: 199 us -> 179 us (0.90)
  waiting for transfers between devices: 64.2 us -> 48.2 us
  other arithmetic: 6.22 us -> 2.19 us
  starting transfers between devices: 39.6 us -> 43.2 us
  Pallas kernels: 21.3 us -> 18.8 us
  matrix products: 2.39 us -> 0.38 us
    all_to_all x1, waiting for transfers between devices: 28.1 us -> 8.77 us  [local(): back = lax.all_to_all(terms, ('y', 'sp'), 0, 0, tiled=True)]
    ppermute x1 -> x2, waiting for transfers between devices: 0.01 us -> 9.74 us  [the longest x1 9.73 us: local(): across_mine = lax.ppermute(mine, 'y', chip)]
    all_to_all x1, waiting for transfers between devices: 6.75 us -> 0.39 us  [local(): final = lax.all_to_all(payload, 'sp', 0, 0, tiled=True)]
    unnamed x3, other arithmetic: 3.4 us -> 0.12 us
    ppermute x1 -> x2, starting transfers between devices: 3.19 us -> 6.45 us  [the longest x1 3.24 us: local(): across_theirs = lax.ppermute(across_mine, 'core', core)]
    pallas_call x8 -> x7, Pallas kernels: 21.3 us -> 18.8 us  [call(): pl.pallas_call(body, out_shape=out, in_specs=specs if specs else [pl.Bloc...]
    dot_general x2, matrix products: 2.39 us -> 0.38 us  [dot(): lax.dot_general(a, b, (((ca,), (cb,)), ((), ())), preferred_element_type=...]
    unnamed x28 -> x34, local copies, waits for them, and re-layouts: 3.43 us -> 4.55 us
  transfers between devices with their start and end apart: 8 -> 9, of which waited for: 5 -> 6; matrix products, arithmetic and copies ran while one was open for 5% -> 2% of each run, Pallas kernels for 5% -> 5%
where the time goes in v3:
time: 179 us; the launch traced here: 178 us
  blocking collectives  58.9 us (33%)
  waiting for transfers between devices  48.2 us (27%)
  starting transfers between devices  43.2 us (24%)
  Pallas kernels  18.8 us (11%)
  local copies, waits for them, and re-layouts  5.32 us (3%)
  other arithmetic  2.19 us (1%)
    all_to_all x1, blocking collectives, local(): lax.all_to_all(rows.reshape(sp_count, 8, width), 'sp', 0, 0, tiled=True)  40 us
    ppermute x3, waiting for transfers between devices, local(): across.append(lax.ppermute(w, 'y', chip))  29.3 us
    all_gather x1, blocking collectives, local(): low = lax.all_gather(share, ('y', 'core'), axis=0)  18.8 us
    pallas_call x7, Pallas kernels, call(): pl.pallas_call(body, out_shape=out, in_specs=specs if specs else [pl.Bloc...  18.8 us
    all_to_all x1, starting transfers between devices, local(): back = lax.all_to_all(terms, ('y', 'sp'), 0, 0, tiled=True)  14 us
    ppermute x1, waiting for transfers between devices, local(): across_mine = lax.ppermute(mine, 'y', chip)  9.73 us
    all_to_all x1, waiting for transfers between devices, local(): back = lax.all_to_all(terms, ('y', 'sp'), 0, 0, tiled=True)  8.77 us
    ppermute x3, starting transfers between devices, local(): across.append(lax.ppermute(w, 'y', chip))  8.49 us
  transfers between devices with their start and end apart: 9, of which 6 were waited for; matrix products, arithmetic and copies ran while one was open for 2% of the time, Pallas kernels for 5%

profile of v3, /device:TPU:1, one launch (start us, length us, event | category | flops | bytes accessed | tf_op | source)
XLA Modules:
  0.0 177.8 jit_solution(2623294969630090913)
XLA Ops:
  0.6 3.0 %shard_map.199 = bf16[256,2048]{1,0:T(8,128)(2,1)} custom-call(s32[2,128]{1,0:T(2,128)} %bitcast.54, f32[2,128]{1,0:T(2,128)} %bitcast.67, bf16[128,2048]{1,0:T(8,128)(2,1)} %stream_ref.1, bf16[128,2048]{1,0:T(8,128)(2,1)} %cot_ref.1), custom_call_target="tpu_custom_call" | custom-call | flops 268435456 | bytes 1048576 | tf_op jit(solution)/shard_map/pallas_call | solution.py:24
  3.7 40.0 %all_to_all.15 = bf16[32,8,2048]{2,1,0:T(8,128)(2,1)S(1)} all-to-all(bf16[32,8,2048]{2,1,0:T(8,128)(2,1)} %bitcast.65), channel_id=1, replica_groups=mesh['sp'=32,'y'=8,'core'=2] {'sp'}, dimensions={0} | all-to-all | bytes 2097152 | tf_op jit(solution)/shard_map/all_to_all | solution.py:312
  43.7 4.7 %collective-permute-start = (bf16[256,2048]{1,0:T(8,128)(2,1)S(1)}, bf16[256,2048]{1,0:T(8,128)(2,1)S(1)}, u32[]{:S(2)}, u32[]{:S(2)}) collective-permute-start(bf16[256,2048]{1,0:T(8,128)(2,1)S(1)} %bitcast.47), channel_id=1, source_target_pairs={{0,1},{1,0},{2,3},{3,2},{4,5},{5,4},{6,7},{7,6},{8,9},{9,8},{10,11... | collective-permute-start | bytes 3145736 | tf_op jit(solution)/shard_map/ppermute | solution.py:314
  48.4 0.0 copy-done.5
  48.4 3.2 %collective-permute-start.3 = (bf16[2048,128]{1,0:T(8,128)(2,1)S(1)}, bf16[2048,128]{1,0:T(8,128)(2,1)S(1)}, u32[]{:S(2)}, u32[]{:S(2)}) collective-permute-start(bf16[2048,128]{1,0:T(8,128)(2,1)S(1)} %bitcast.56), channel_id=1, source_target_pairs={{0,2},{2,0},{4,6},{6,4},{8,10},{10,8},{12,14},{14,12},{1,3},{3,1},... | collective-permute-start | bytes 1572872 | tf_op jit(solution)/shard_map/ppermute | solution.py:299
  51.7 0.0 copy-done.6
  51.7 2.1 %collective-permute-start.4 = (bf16[2048,128]{1,0:T(8,128)(2,1)S(1)}, bf16[2048,128]{1,0:T(8,128)(2,1)S(1)}, u32[]{:S(2)}, u32[]{:S(2)}) collective-permute-start(bf16[2048,128]{1,0:T(8,128)(2,1)S(1)} %bitcast.59), channel_id=1, source_target_pairs={{0,2},{2,0},{4,6},{6,4},{8,10},{10,8},{12,14},{14,12},{1,3},{3,1},... | collective-permute-start | bytes 1572872 | tf_op jit(solution)/shard_map/ppermute | solution.py:299
  53.7 0.0 copy-done.8
  53.8 0.0 copy-start.15
  53.8 3.2 %collective-permute-start.5 = (bf16[128,2048]{1,0:T(8,128)(2,1)S(1)}, bf16[128,2048]{1,0:T(8,128)(2,1)S(1)}, u32[]{:S(2)}, u32[]{:S(2)}) collective-permute-start(bf16[128,2048]{1,0:T(8,128)(2,1)S(1)} %bitcast.62), channel_id=1, source_target_pairs={{0,2},{2,0},{4,6},{6,4},{8,10},{10,8},{12,14},{14,12},{1,3},{3,1},... | collective-permute-start | bytes 1572872 | tf_op jit(solution)/shard_map/ppermute | solution.py:299
  57.0 6.8 %collective-permute-done.3.refs_3_ = bf16[2048,128]{1,0:T(8,128)(2,1)S(1)} collective-permute-done((bf16[2048,128]{1,0:T(8,128)(2,1)S(1)}, bf16[2048,128]{1,0:T(8,128)(2,1)S(1)}, u32[]{:S(2)}, u32[]{:S(2)}) %collective-permute-start.3) | collective-permute-done | bytes 524320 | tf_op jit(solution)/shard_map/ppermute | solution.py:299
  63.8 11.2 %collective-permute-done.4.refs_4_ = bf16[2048,128]{1,0:T(8,128)(2,1)S(1)} collective-permute-done((bf16[2048,128]{1,0:T(8,128)(2,1)S(1)}, bf16[2048,128]{1,0:T(8,128)(2,1)S(1)}, u32[]{:S(2)}, u32[]{:S(2)}) %collective-permute-start.4) | collective-permute-done | bytes 524320 | tf_op jit(solution)/shard_map/ppermute | solution.py:299
  75.0 11.2 %collective-permute-done.5.refs_5_ = bf16[128,2048]{1,0:T(8,128)(2,1)S(1)} collective-permute-done((bf16[128,2048]{1,0:T(8,128)(2,1)S(1)}, bf16[128,2048]{1,0:T(8,128)(2,1)S(1)}, u32[]{:S(2)}, u32[]{:S(2)}) %collective-permute-start.5) | collective-permute-done | bytes 524320 | tf_op jit(solution)/shard_map/ppermute | solution.py:299
  86.3 0.0 collective-permute-done.rb_ref
  86.3 5.3 %shard_map.200 = (bf16[8,256,128]{2,1,0:T(8,128)(2,1)S(1)}, bf16[8,256,128]{2,1,0:T(8,128)(2,1)}, bf16[2,256,384]{2,1,0:T(8,128)(2,1)S(1)}) custom-call(bf16[256,2048]{1,0:T(8,128)(2,1)S(1)} %bitcast.48, bf16[256,2048]{1,0:T(8,128)(2,1)S(1)} %collective-permute-done.rb_ref, bf16[2048,128]{1,0:T(8,128)(2,1)S(1)} %bitcast.57, bf16[2048,128]{1,0:T(8,128)(2,1)S(1)} %bitcast.60, ...), custom_call_target="tpu_custom_call" | custom-call | flops 2147483648 | bytes 1048576 | tf_op jit(solution)/shard_map/pallas_call | solution.py:24
  91.5 0.0 copy-start.10
  91.6 0.7 copy-done.10
  92.3 2.9 %collective-permute-start.6 = (bf16[8,256,128]{2,1,0:T(8,128)(2,1)}, bf16[8,256,128]{2,1,0:T(8,128)(2,1)}, u32[]{:S(2)}, u32[]{:S(2)}) collective-permute-start(bf16[8,256,128]{2,1,0:T(8,128)(2,1)} %get-tuple-element.23), channel_id=1, source_target_pairs={{0,1},{1,0},{2,3},{3,2},{4,5},{5,4},{6,7},{7,6},{8,9},{9,8},{10,11... | collective-permute-start | bytes 1572872 | tf_op jit(solution)/shard_map/ppermute | solution.py:338
  95.2 0.0 copy-done.16
  95.2 0.0 copy-start.14
  95.2 3.2 %collective-permute-start.1 = (bf16[256,2048]{1,0:T(8,128)(2,1)S(1)}, bf16[256,2048]{1,0:T(8,128)(2,1)}, u32[]{:S(2)}, u32[]{:S(2)}) collective-permute-start(bf16[256,2048]{1,0:T(8,128)(2,1)S(1)} %bitcast.49), channel_id=1, source_target_pairs={{0,2},{2,0},{4,6},{6,4},{8,10},{10,8},{12,14},{14,12},{1,3},{3,1},... | collective-permute-start | bytes 3145736 | tf_op jit(solution)/shard_map/ppermute | solution.py:315
  98.5 0.2 bitcast_dynamic-update-slice_fusion.2
  98.7 0.0 collective-permute-done.6
  98.7 2.0 %add_convert_fusion = bf16[8,256,128]{2,1,0:T(8,128)(2,1)} fusion(bf16[8,256,128]{2,1,0:T(8,128)(2,1)} %collective-permute-done.6, bf16[8,256,128]{2,1,0:T(8,128)(2,1)S(1)} %get-tuple-element.22), kind=kLoop, calls=%fused_computation.8 | loop fusion | flops 1048576 | bytes 1572864 | tf_op jit(solution)/shard_map/convert_element_type | solution.py:339
  100.8 14.0 %all-to-all-start.1 = ((bf16[256,8,128]{2,1,0:T(8,128)(2,1)}), bf16[256,8,128]{2,1,0:T(8,128)(2,1)S(1)}, u32[]{:S(2)}, u32[]{:S(2)}) async-start(bf16[256,8,128]{2,1,0:T(8,128)(2,1)} %bitcast.66), calls=%async_computation.1 | async-start | bytes 1048576 | tf_op jit(solution)/shard_map/all_to_all | solution.py:341
  114.8 0.2 fusion.10
  115.0 9.7 %collective-permute-done.1.rc_ref = bf16[256,2048]{1,0:T(8,128)(2,1)} collective-permute-done((bf16[256,2048]{1,0:T(8,128)(2,1)S(1)}, bf16[256,2048]{1,0:T(8,128)(2,1)}, u32[]{:S(2)}, u32[]{:S(2)}) %collective-permute-start.1) | collective-permute-done | bytes 1048608 | tf_op jit(solution)/shard_map/ppermute | solution.py:315
  124.8 3.2 %collective-permute-start.2 = (bf16[256,2048]{1,0:T(8,128)(2,1)}, bf16[256,2048]{1,0:T(8,128)(2,1)}, u32[]{:S(2)}, u32[]{:S(2)}) collective-permute-start(bf16[256,2048]{1,0:T(8,128)(2,1)} %collective-permute-done.1.rc_ref), channel_id=1, source_target_pairs={{0,1},{1,0},{2,3},{3,2},{4,5},{5,4},{6,7},{7,6},{8,9},{9,8},{10,11... | collective-permute-start | bytes 3145736 | tf_op jit(solution)/shard_map/ppermute | solution.py:316
  128.0 0.1 bitcast_dynamic-update-slice_fusion.1
  128.1 0.7 copy-done.4
  128.8 0.3 shard_map.202.pick_ref
  129.1 0.8 constant_dynamic-slice_fusion.own_ref
  129.9 8.8 %all-to-all-done.1 = bf16[256,8,128]{2,1,0:T(8,128)(2,1)S(1)} async-done(((bf16[256,8,128]{2,1,0:T(8,128)(2,1)}), bf16[256,8,128]{2,1,0:T(8,128)(2,1)S(1)}, u32[]{:S(2)}, u32[]{:S(2)}) %all-to-all-start.1) | async-done | bytes 524320 | tf_op jit(solution)/shard_map/all_to_all | solution.py:341
  138.7 0.3 shard_map.203
  138.9 0.0 copy-start
  139.0 0.0 copy-start.1
  139.0 18.8 %all-gather = bf16[2048,128]{1,0:T(8,128)(2,1)S(1)} all-gather(bf16[128,128]{1,0:T(8,128)(2,1)S(1)} %shard_map.203), channel_id=2, replica_groups=mesh['sp'=32,'y'=8,'core'=2] {'y','core'}, dimensions={0}, use_global_device_ids=true | all-gather | bytes 557056 | tf_op jit(solution)/shard_map/all_gather | solution.py:347
  157.8 0.0 copy-done.1
  157.8 1.9 %shard_map.204 = (bf16[32,24,128]{2,1,0:T(8,128)(2,1)}, f32[32,128]{1,0:T(8,128)}, f32[32,128]{1,0:T(8,128)S(1)}, f32[32,128]{1,0:T(8,128)S(1)}) custom-call(bf16[16,128,128]{2,1,0:T(8,128)(2,1)S(1)} %bitcast.46, bf16[32,2048]{1,0:T(8,128)(2,1)S(1)} %bitcast.51, bf16[32,128]{1,0:T(8,128)(2,1)S(1)} %copy-done.1, ...), custom_call_target="tpu_custom_call" | custom-call | flops 134217728 | bytes 1048576 | tf_op jit(solution)/shard_map/pallas_call | solution.py:24
  159.7 6.6 %all-to-all-start.2 = ((bf16[32,24,128]{2,1,0:T(8,128)(2,1)}), bf16[32,24,128]{2,1,0:T(8,128)(2,1)S(1)}, u32[]{:S(2)}, u32[]{:S(2)}) async-start(bf16[32,24,128]{2,1,0:T(8,128)(2,1)} %get-tuple-element.24), calls=%async_computation.2 | async-start | bytes 393216 | tf_op jit(solution)/shard_map/all_to_all | solution.py:362
  166.3 0.0 collective-permute-done.2.rd_ref
  166.3 0.0 copy-start.7
  166.4 1.0 copy-done.7
  167.4 1.0 copy-done.9
  168.4 1.0 copy-done.11
  169.4 7.0 %shard_map.201 = (bf16[2048,128]{1,0:T(8,128)(2,1)}, bf16[2048,128]{1,0:T(8,128)(2,1)}, bf16[128,2048]{1,0:T(8,128)(2,1)}) custom-call(bf16[256,2048]{1,0:T(8,128)(2,1)S(1)} %bitcast.50, bf16[256,2048]{1,0:T(8,128)(2,1)S(1)} %collective-permute-done.rb_ref, bf16[256,2048]{1,0:T(8,128)(2,1)} %collective-permute-done.1.rc_ref, ...), custom_call_target="tpu_custom_call" | custom-call | flops 2147483648 | bytes 1048576 | tf_op jit(solution)/shard_map/pallas_call | solution.py:24
  176.4 0.4 all-to-all-done.2.recv_ref
  176.8 1.0 shard_map.205
  (23 shorter events, 0.1 us)
Async XLA Ops:
  3.7 44.8 %copy-start.5 = (bf16[1,2048,128]{2,1,0:T(8,128)(2,1)S(1)}, bf16[1,2048,128]{2,1,0:T(8,128)(2,1)}, u32[]{:S(2)}) copy-start(bf16[1,2048,128]{2,1,0:T(8,128)(2,1)} %param.20) | copy-start | bytes 1572868
  3.7 48.0 %copy-start.6 = (bf16[1,2048,128]{2,1,0:T(8,128)(2,1)S(1)}, bf16[1,2048,128]{2,1,0:T(8,128)(2,1)}, u32[]{:S(2)}) copy-start(bf16[1,2048,128]{2,1,0:T(8,128)(2,1)} %param.21) | copy-start | bytes 1572868
  3.7 50.1 %copy-start.8 = (bf16[1,128,2048]{2,1,0:T(8,128)(2,1)S(1)}, bf16[1,128,2048]{2,1,0:T(8,128)(2,1)}, u32[]{:S(2)}) copy-start(bf16[1,128,2048]{2,1,0:T(8,128)(2,1)} %param.22) | copy-start | bytes 1572868
  43.7 42.6 %collective-permute-start = (bf16[256,2048]{1,0:T(8,128)(2,1)S(1)}, bf16[256,2048]{1,0:T(8,128)(2,1)S(1)}, u32[]{:S(2)}, u32[]{:S(2)}) collective-permute-start(bf16[256,2048]{1,0:T(8,128)(2,1)S(1)} %bitcast.47), channel_id=1, source_target_pairs={{0,1},{1,0},{2,3},{3,2},{4,5},{5,4},{6,7},{7,6},{8,9},{9,8},{10,11... | collective-permute-start | bytes 3145736 | tf_op jit(solution)/shard_map/ppermute | solution.py:314
  48.4 15.4 %collective-permute-start.3 = (bf16[2048,128]{1,0:T(8,128)(2,1)S(1)}, bf16[2048,128]{1,0:T(8,128)(2,1)S(1)}, u32[]{:S(2)}, u32[]{:S(2)}) collective-permute-start(bf16[2048,128]{1,0:T(8,128)(2,1)S(1)} %bitcast.56), channel_id=1, source_target_pairs={{0,2},{2,0},{4,6},{6,4},{8,10},{10,8},{12,14},{14,12},{1,3},{3,1},... | collective-permute-start | bytes 1572872 | tf_op jit(solution)/shard_map/ppermute | solution.py:299
  51.7 23.4 %collective-permute-start.4 = (bf16[2048,128]{1,0:T(8,128)(2,1)S(1)}, bf16[2048,128]{1,0:T(8,128)(2,1)S(1)}, u32[]{:S(2)}, u32[]{:S(2)}) collective-permute-start(bf16[2048,128]{1,0:T(8,128)(2,1)S(1)} %bitcast.59), channel_id=1, source_target_pairs={{0,2},{2,0},{4,6},{6,4},{8,10},{10,8},{12,14},{14,12},{1,3},{3,1},... | collective-permute-start | bytes 1572872 | tf_op jit(solution)/shard_map/ppermute | solution.py:299
  53.8 44.7 %copy-start.15 = (f32[32,128]{1,0:T(8,128)S(1)}, f32[32,128]{1,0:T(8,128)}, u32[]{:S(2)}) copy-start(f32[32,128]{1,0:T(8,128)} %param.31) | copy-start | bytes 49156
  53.8 32.5 %collective-permute-start.5 = (bf16[128,2048]{1,0:T(8,128)(2,1)S(1)}, bf16[128,2048]{1,0:T(8,128)(2,1)S(1)}, u32[]{:S(2)}, u32[]{:S(2)}) collective-permute-start(bf16[128,2048]{1,0:T(8,128)(2,1)S(1)} %bitcast.62), channel_id=1, source_target_pairs={{0,2},{2,0},{4,6},{6,4},{8,10},{10,8},{12,14},{14,12},{1,3},{3,1},... | collective-permute-start | bytes 1572872 | tf_op jit(solution)/shard_map/ppermute | solution.py:299
  86.3 8.9 %copy-start.16 = (f32[32]{0:T(128)S(1)}, f32[32]{0:T(128)}, u32[]{:S(2)}) copy-start(f32[32]{0:T(128)} %param.30) | copy-start | bytes 388
  86.3 12.2 %copy-start.12 = (bf16[32,128]{1,0:T(8,128)(2,1)S(1)}, bf16[32,128]{1,0:T(8,128)(2,1)}, u32[]{:S(2)}) copy-start(bf16[32,128]{1,0:T(8,128)(2,1)} %param.25) | copy-start | bytes 24580
  91.5 0.7 copy-start.10
  92.3 6.2 %copy-start.2 = (bf16[1,32,32]{2,1,0:T(8,128)(2,1)S(1)}, bf16[1,32,32]{2,1,0:T(8,128)(2,1)}, u32[]{:S(2)}) copy-start(bf16[1,32,32]{2,1,0:T(8,128)(2,1)} %param.28) | copy-start | bytes 6148
  92.3 6.4 %collective-permute-start.6 = (bf16[8,256,128]{2,1,0:T(8,128)(2,1)}, bf16[8,256,128]{2,1,0:T(8,128)(2,1)}, u32[]{:S(2)}, u32[]{:S(2)}) collective-permute-start(bf16[8,256,128]{2,1,0:T(8,128)(2,1)} %get-tuple-element.23), channel_id=1, source_target_pairs={{0,1},{1,0},{2,3},{3,2},{4,5},{5,4},{6,7},{7,6},{8,9},{9,8},{10,11... | collective-permute-start | bytes 1572872 | tf_op jit(solution)/shard_map/ppermute | solution.py:338
  95.2 3.5 %copy-start.14 = (bf16[32,128]{1,0:T(8,128)(2,1)S(1)}, bf16[32,128]{1,0:T(8,128)(2,1)}, u32[]{:S(2)}) copy-start(bf16[32,128]{1,0:T(8,128)(2,1)} %param.26) | copy-start | bytes 24580
  95.2 29.5 %collective-permute-start.1 = (bf16[256,2048]{1,0:T(8,128)(2,1)S(1)}, bf16[256,2048]{1,0:T(8,128)(2,1)}, u32[]{:S(2)}, u32[]{:S(2)}) collective-permute-start(bf16[256,2048]{1,0:T(8,128)(2,1)S(1)} %bitcast.49), channel_id=1, source_target_pairs={{0,2},{2,0},{4,6},{6,4},{8,10},{10,8},{12,14},{14,12},{1,3},{3,1},... | collective-permute-start | bytes 3145736 | tf_op jit(solution)/shard_map/ppermute | solution.py:315
  100.8 14.1 %copy-start.3 = (bf16[1,32,32]{2,1,0:T(8,128)(2,1)S(1)}, bf16[1,32,32]{2,1,0:T(8,128)(2,1)}, u32[]{:S(2)}) copy-start(bf16[1,32,32]{2,1,0:T(8,128)(2,1)} %param.29) | copy-start | bytes 6148
  100.8 14.1 %copy-start.13 = (f32[32,128]{1,0:T(8,128)S(1)}, f32[32,128]{1,0:T(8,128)}, u32[]{:S(2)}) copy-start(f32[32,128]{1,0:T(8,128)} %param.27) | copy-start | bytes 49156
  100.8 37.9 %all-to-all-start.1 = ((bf16[256,8,128]{2,1,0:T(8,128)(2,1)}), bf16[256,8,128]{2,1,0:T(8,128)(2,1)S(1)}, u32[]{:S(2)}, u32[]{:S(2)}) async-start(bf16[256,8,128]{2,1,0:T(8,128)(2,1)} %bitcast.66), calls=%async_computation.1 | async-start | bytes 1048576 | tf_op jit(solution)/shard_map/all_to_all | solution.py:341
  124.8 41.6 %collective-permute-start.2 = (bf16[256,2048]{1,0:T(8,128)(2,1)}, bf16[256,2048]{1,0:T(8,128)(2,1)}, u32[]{:S(2)}, u32[]{:S(2)}) collective-permute-start(bf16[256,2048]{1,0:T(8,128)(2,1)} %collective-permute-done.1.rc_ref), channel_id=1, source_target_pairs={{0,1},{1,0},{2,3},{3,2},{4,5},{5,4},{6,7},{7,6},{8,9},{9,8},{10,11... | collective-permute-start | bytes 3145736 | tf_op jit(solution)/shard_map/ppermute | solution.py:316
  128.1 0.7 copy-start.4
  138.9 18.9 %copy-start = (bf16[2048,32]{0,1:T(8,128)(2,1)S(1)}, bf16[2048,32]{0,1:T(8,128)(2,1)}, u32[]{:S(2)}) copy-start(bf16[2048,32]{0,1:T(8,128)(2,1)} %param.23) | copy-start | bytes 393220
  139.0 18.8 %copy-start.1 = (bf16[32,128]{1,0:T(8,128)(2,1)S(1)}, bf16[32,128]{1,0:T(8,128)(2,1)}, u32[]{:S(2)}) copy-start(bf16[32,128]{1,0:T(8,128)(2,1)} %mixed_ref.1) | copy-start | bytes 24580
  159.7 17.1 %all-to-all-start.2 = ((bf16[32,24,128]{2,1,0:T(8,128)(2,1)}), bf16[32,24,128]{2,1,0:T(8,128)(2,1)S(1)}, u32[]{:S(2)}, u32[]{:S(2)}) async-start(bf16[32,24,128]{2,1,0:T(8,128)(2,1)} %get-tuple-element.24), calls=%async_computation.2 | async-start | bytes 393216 | tf_op jit(solution)/shard_map/all_to_all | solution.py:362
  166.3 1.0 copy-start.7
  167.4 1.0 copy-start.9
  168.4 1.0 copy-start.11
